TPU v7x, 32 devices: a whole 2x2x4 slice. The times are simulated.
32 devices in a mesh: sp: 8 (over z, y), tp: 4 (over x, core).
Axes of the slice: x: 2, y: 2, z: 4, core: 2. Of those that a mesh axis runs over, the one named last changes fastest.
Arguments:
- activations: bfloat16 [4096, 2048], P('sp', 'tp'), may hold values from -250 to 250
- norm_gain: bfloat16 [2048], P('tp'), may hold values from 0.099609375 to 1.8984375
- pool_weight: bfloat16 [2048, 1024], P('sp', 'tp'), may hold values from -0.125 to 0.125
- gate_weight: bfloat16 [2048, 1024], P('sp', 'tp'), may hold values from -0.125 to 0.125
- value_weight: bfloat16 [2048, 1024], P('sp', 'tp'), may hold values from -0.125 to 0.125
- key_weight: bfloat16 [2048, 256], P('sp', 'tp'), may hold values from -0.125 to 0.125
- read_weight: bfloat16 [2048, 256], P('sp', 'tp'), may hold values from -0.125 to 0.125
- step_weight: bfloat16 [2048, 16], P('sp', 'tp'), may hold values from -0.125 to 0.125
- pool_mix: bfloat16 [4, 256, 256], P('tp'), may hold values from -0.375 to 0.375
- pool_scale: float32 [1024], P('tp'), may hold values from 0.1 to 1.9
- taps_value: float32 [4, 1024], P(None, 'tp'), may hold values from -3 to 3
- taps_key: float32 [4, 256], P(None, 'tp'), may hold values from -3 to 3
- taps_read: float32 [4, 256], P(None, 'tp'), may hold values from -3 to 3
- step_bias: float32 [16], P('tp'), may hold values from -1 to 1
- decay_log: float32 [16], P('tp')
- decay_extra: float32 [4096, 16], P('sp', 'tp'), may hold values from -1 to 0
- skip_scale: float32 [16], P('tp'), may hold values from 0.5 to 2
- state_gain: float32 [1024], P('tp'), may hold values from 0.1 to 1.9
- out_pool_weight: bfloat16 [1024, 2048], P('tp', 'sp'), may hold values from -0.125 to 0.125
- out_state_weight: bfloat16 [1024, 2048], P('tp', 'sp'), may hold values from -0.125 to 0.125
Outputs:
- mixed: bfloat16 [4096, 2048], P('sp', 'tp')
All inputs are finite; a program needn't handle non-finite values.
Results may differ from a plain program's by a relative error of at most 0.007.
Values may be sent and summed in bfloat16 or wider, within the bound.
A program may use at most 64 MiB of HBM per device.

v0:
```python
import functools

import jax
import jax.numpy as jnp
from jax import lax
from jax.experimental import pallas as pl
from jax.experimental.pallas import tpu as pltpu
from jax.sharding import PartitionSpec as P

SSM_STATE = 64
POOL_GROUPS = 4
SCAN_BLOCK = 128
MIX_W = 1024


EPSILON = 1e-06
HIGH = lax.Precision.HIGHEST


def shifted(value, axis, steps):
    count = lax.axis_size(axis)
    leading, last = (max(0, -steps), min(count, count - steps))
    return lax.ppermute(value, axis, [(source, source + steps) for source in range(leading, last)])


def carried_in(part, axis, combine, identity):
    place = lax.axis_index(axis)
    gathered = jax.tree.map(lambda a: lax.all_gather(a, axis), part)
    state = jax.tree.map(lambda a, e: jnp.zeros_like(a) + jnp.asarray(e, a.dtype), part, identity)

    def one(step, state):
        return combine(
            state, jax.tree.map(lambda a: lax.dynamic_index_in_dim(a, step, 0, False), gathered)
        )

    return lax.fori_loop(0, place, one, state)


def backward_kernel(extended, taps):
    width = taps.shape[0]
    length = extended.shape[0] - (width - 1)
    widened_rows = extended.astype(jnp.float32)
    total = jnp.zeros((length, extended.shape[1]), jnp.float32)
    for offset in range(width):
        total = total + taps[offset][None, :] * widened_rows[offset : offset + length]
    return jax.nn.silu(total).astype(jnp.bfloat16)


def combine_states(preceding_token, later):
    return (preceding_token[0] * later[0], preceding_token[1] * later[0][:, None, None] + later[1])


def local(
    activations,
    norm_gain,
    pool_weight,
    gate_weight,
    value_weight,
    key_weight,
    read_weight,
    step_weight,
    pool_mix,
    pool_scale,
    taps_value,
    taps_key,
    taps_read,
    step_bias,
    decay_log,
    decay_extra,
    skip_scale,
    state_gain,
    out_pool_weight,
    out_state_weight,
):
    length = activations.shape[0]
    cluster_span = pool_weight.shape[1]
    local_mix = gate_weight.shape[1]
    local_state = key_weight.shape[1]
    local_heads = step_weight.shape[1]
    joined = jnp.concatenate(
        [pool_weight, gate_weight, value_weight, key_weight, read_weight, step_weight], axis=1
    )
    in_weight = lax.all_gather(joined, "sp", axis=0, tiled=True)
    whole, gains = (
        lax.all_gather(activations, "tp", axis=1, tiled=True),
        lax.all_gather(norm_gain, "tp", axis=0, tiled=True),
    )
    widened_rows = whole.astype(jnp.float32)
    normed = (
        widened_rows
        * lax.rsqrt(jnp.mean(widened_rows * widened_rows, axis=-1, keepdims=True) + EPSILON)
        * gains.astype(jnp.float32)
    ).astype(jnp.bfloat16)
    projected = jnp.dot(normed, in_weight, preferred_element_type=jnp.float32)
    column = 0
    pool_in = projected[:, column : column + cluster_span].astype(jnp.bfloat16)
    column = column + cluster_span
    gate_in = projected[:, column : column + local_mix].astype(jnp.bfloat16)
    column = column + local_mix
    raw_value = projected[:, column : column + local_mix].astype(jnp.bfloat16)
    column = column + local_mix
    raw_key = projected[:, column : column + local_state].astype(jnp.bfloat16)
    column = column + local_state
    raw_read = projected[:, column : column + local_state].astype(jnp.bfloat16)
    column = column + local_state
    step_raw = projected[:, column : column + local_heads]
    raw_joined = jnp.concatenate([raw_value, raw_key, raw_read], axis=1)
    reach = 2**POOL_GROUPS - 1
    width = taps_value.shape[0]
    prior_pool, prior_joined = shifted(
        (pool_in[length - reach :], raw_joined[length - width + 1 :]), "sp", 1
    )
    group = lax.axis_index("tp")
    running = jnp.concatenate([prior_pool, pool_in], axis=0).astype(jnp.float32)
    levels = []
    for level in range(POOL_GROUPS):
        stride = 2**level
        running = running[stride:] + running[:-stride]
        levels.append(running[running.shape[0] - length :])
    window_sum = lax.dynamic_index_in_dim(jnp.stack(levels), group, 0, keepdims=False)
    window = jnp.exp2((group + 1).astype(jnp.float32))
    position = (lax.axis_index("sp") * length + jnp.arange(length, dtype=jnp.int32)).astype(
        jnp.float32
    )
    counts = jnp.minimum(position + 1.0, window)
    pooled = (window_sum / counts[:, None] - pool_in.astype(jnp.float32)).astype(jnp.bfloat16)
    pool_out = (
        jnp.dot(pooled, pool_mix[0], preferred_element_type=jnp.float32) * pool_scale
    ).astype(jnp.bfloat16)
    all_taps = jnp.concatenate([taps_value, taps_key, taps_read], axis=1)
    convolved = backward_kernel(jnp.concatenate([prior_joined, raw_joined], axis=0), all_taps)
    head_value = convolved[:, :local_mix]
    key_vectors = convolved[:, local_mix : local_mix + local_state]
    read_vectors = convolved[:, local_mix + local_state :]
    head_dim = local_mix // local_heads
    groups_here = local_state // SSM_STATE
    repeat = local_heads // groups_here
    blocks = length // SCAN_BLOCK
    step_size = jax.nn.softplus(step_raw + step_bias)
    log_decay = -jnp.exp(decay_log) * step_size + decay_extra
    value_heads = head_value.astype(jnp.float32).reshape(length, local_heads, head_dim)
    value_blocks = value_heads.reshape(blocks, SCAN_BLOCK, local_heads, head_dim)
    key_blocks = jnp.repeat(
        key_vectors.astype(jnp.float32).reshape(length, groups_here, SSM_STATE), repeat, axis=1
    ).reshape(blocks, SCAN_BLOCK, local_heads, SSM_STATE)
    read_blocks = jnp.repeat(
        read_vectors.astype(jnp.float32).reshape(length, groups_here, SSM_STATE), repeat, axis=1
    ).reshape(blocks, SCAN_BLOCK, local_heads, SSM_STATE)
    step_blocks = step_size.reshape(blocks, SCAN_BLOCK, local_heads)
    running_decay = jnp.cumsum(log_decay.reshape(blocks, SCAN_BLOCK, local_heads), axis=1)
    lower = jnp.arange(SCAN_BLOCK)[:, None] >= jnp.arange(SCAN_BLOCK)[None, :]
    gaps = jnp.where(
        lower[None, :, :, None],
        running_decay[:, :, None, :] - running_decay[:, None, :, :],
        -jnp.inf,
    )
    weights = jnp.einsum("blhn,bshn->blsh", read_blocks, key_blocks, precision=HIGH) * jnp.exp(gaps)
    scaled_value = value_blocks * step_blocks[..., None]
    inner = jnp.einsum("blsh,bshp->blhp", weights, scaled_value, precision=HIGH)
    block_ends = running_decay[:, -1, :]
    trailing = jnp.exp(block_ends[:, None, :] - running_decay)
    fresh = jnp.einsum("bshn,bsh,bshp->bhpn", key_blocks, trailing, scaled_value, precision=HIGH)

    def advance(carry, inputs):
        block_decay, block_state = inputs
        return (carry * block_decay[:, None, None] + block_state, carry)

    local_total, prefix = lax.scan(
        advance,
        jnp.zeros((local_heads, head_dim, SSM_STATE), jnp.float32),
        (jnp.exp(block_ends), fresh),
    )
    offsets = jnp.cumsum(block_ends, axis=0) - block_ends
    device_decay = jnp.exp(offsets[-1] + block_ends[-1])
    incoming_decay, incoming = carried_in(
        (device_decay, local_total),
        "sp",
        combine_states,
        (jnp.ones_like(device_decay), jnp.zeros_like(local_total)),
    )
    from_device = running_decay + offsets[:, None, :]
    local_off = (
        jnp.einsum("blhn,bhpn->blhp", read_blocks, prefix, precision=HIGH)
        * jnp.exp(running_decay)[..., None]
    )
    far_off = (
        jnp.einsum("blhn,hpn->blhp", read_blocks, incoming, precision=HIGH)
        * jnp.exp(from_device)[..., None]
    )
    scan_out = (inner + local_off + far_off).reshape(length, local_heads, head_dim) + skip_scale[
        None, :, None
    ] * value_heads
    gated = scan_out.reshape(length, local_mix) * jax.nn.silu(gate_in.astype(jnp.float32))
    gate_squares = lax.psum(jnp.sum(gated * gated, axis=-1), "tp")
    state_out = (gated * lax.rsqrt(gate_squares / MIX_W + EPSILON)[:, None] * state_gain).astype(
        jnp.bfloat16
    )
    branch_rows = jnp.concatenate([pool_out, state_out], axis=1)
    out_weight = jnp.concatenate([out_pool_weight, out_state_weight], axis=0)
    terms = jnp.dot(
        branch_rows,
        lax.all_gather(out_weight, "sp", axis=1, tiled=True),
        preferred_element_type=jnp.float32,
    )
    result = lax.psum_scatter(terms, "tp", scatter_dimension=1, tiled=True)
    return result.astype(jnp.bfloat16)


BF = jnp.bfloat16
F32 = jnp.float32
MESH = pl.DeviceIdType.MESH


def flip(index, mask):
    bit = 1
    while bit <= mask:
        if mask & bit:
            index = index + bit - 2 * bit * lax.rem(lax.div(index, bit), 2)
        bit *= 2
    return index


class Stream:
    def __init__(self, axis, place, bits, refs, send_sems, recv_sems, base, started):
        self.axis, self.place, self.bits, self.refs = axis, place, bits, refs
        self.send_sems, self.recv_sems, self.base, self.started = send_sems, recv_sems, base, started

    def via(self, mask):
        return [bit for bit in self.bits if mask & bit][-1]

    def copy(self, mask, bit):
        ref = self.refs(flip(self.place, mask))
        slot = self.base + (mask | bit)
        return pltpu.make_async_remote_copy(
            src_ref=ref, dst_ref=ref, send_sem=self.send_sems.at[slot], recv_sem=self.recv_sems.at[slot],
            device_id={self.axis: flip(self.place, bit)}, device_id_type=MESH,
        )

    def push(self, mask):
        onward = self.bits if mask == 0 else self.bits[self.bits.index(self.via(mask)) + 1 :]
        for bit in sorted(onward):
            c = self.copy(mask, bit)
            c.start()
            self.started.append(c)

    def got(self, mask):
        ref = self.refs(flip(self.place, mask))
        slot = self.base + mask
        pltpu.make_async_remote_copy(
            src_ref=ref, dst_ref=ref, send_sem=self.send_sems.at[slot], recv_sem=self.recv_sems.at[slot],
            device_id={self.axis: flip(self.place, self.via(mask))}, device_id_type=MESH,
        ).wait_recv()
        self.push(mask)


def early_first(size):
    return [m for m in range(2, size) if m // 2 & (m // 2 - 1) == 0 and m > 3]


def bt(a, b, **kw):
    return lax.dot_general(a, b, (((1,), (1,)), ((), ())), preferred_element_type=F32, **kw)


def halves(x):
    top = x.astype(BF)
    return top, (x - top.astype(F32)).astype(BF)


def mixer_kernel(
    S, T,
    act, gain, pool_w, gate_w, value_w, key_w, read_w, step_t, mix, scale, taps_v, taps_k, taps_r,
    bias, dlog, extra_t, skip, sgain, opool, ostate,
    out,
    wbuf, sbuf, obuf, abuf, nbuf, acc, sacc, ext, conv, hsend, hrecv, scan, xs, xr, ssend, srecv,
    brow, psend, precv, pown, qsend, qrecv, expd,
    w_ss, w_rs, s_ss, s_rs, o_ss, o_rs, a_ss, a_rs, h_ss, h_rs, x_ss, x_rs, q_ss, q_rs, p_ss, p_rs, r_ss, r_rs,
):
    n, da = act.shape
    kd = pool_w.shape[0]
    cw = pool_w.shape[1]
    st = key_w.shape[0]
    ncol = wbuf.shape[2]
    blk = SCAN_BLOCK
    blocks = n // blk
    hd = SSM_STATE
    me = lax.axis_index("sp")
    tp = lax.axis_index("tp")
    wbuf[me, :, 0:cw] = pool_w[...]
    wbuf[me, :, cw : 2 * cw] = gate_w[...]
    wbuf[me, :, 2 * cw : 3 * cw] = value_w[...]
    eye_kd = jnp.where(
        lax.broadcasted_iota(jnp.int32, (kd, kd), 0) == lax.broadcasted_iota(jnp.int32, (kd, kd), 1), 1.0, 0.0
    ).astype(BF)
    wbuf[me, :, 3 * cw :] = bt(eye_kd, jnp.concatenate([key_w[...], read_w[...]], axis=0)).astype(BF)
    hp = sbuf.shape[1]
    heads = step_t.shape[0]
    pick = jnp.where(
        lax.broadcasted_iota(jnp.int32, (hp, heads), 0) == lax.broadcasted_iota(jnp.int32, (hp, heads), 1), 1.0, 0.0
    ).astype(F32)
    sbuf[me] = jnp.dot(pick.astype(BF), step_t[...], preferred_element_type=F32).astype(BF)
    abuf[tp, 0:n, :] = act[...]
    abuf[tp, n : n + 16, :] = jnp.broadcast_to(gain[...].astype(F32), (16, da)).astype(BF)

    barrier = pltpu.get_barrier_semaphore()
    for k in range(1, S):
        pl.semaphore_signal(barrier, inc=1, device_id={"sp": lax.rem(me + k, S)}, device_id_type=MESH)
    for k in range(1, T):
        pl.semaphore_signal(barrier, inc=1, device_id={"tp": lax.rem(tp + k, T)}, device_id_type=MESH)
    obuf[me, 0:cw, :] = opool[...]
    obuf[me, cw:, :] = ostate[...]
    pl.semaphore_wait(barrier, S - 1 + T - 1)

    started = []

    def remote(src, dst, ss, rs, **peer):
        c = pltpu.make_async_remote_copy(
            src_ref=src, dst_ref=dst, send_sem=ss, recv_sem=rs, device_id=peer, device_id_type=MESH
        )
        return c

    def send(*a, **k):
        c = remote(*a, **k)
        c.start()
        started.append(c)

    far = [1 << k for k in reversed(range(1, S.bit_length() - 1))]
    late = far + [1]
    early = [1] + far
    cut = -(-kd // 96) * 16
    ocut = cut * 2 * cw // kd
    wq = Stream("sp", me, late, lambda i: wbuf.at[i, pl.ds(cut, kd - cut)], w_ss, w_rs, 0, started)
    wp = Stream("sp", me, early, lambda i: wbuf.at[i, pl.ds(0, cut)], w_ss, w_rs, S, started)
    sq_ = Stream("sp", me, late, lambda i: sbuf.at[i], s_ss, s_rs, 0, started)
    oq = Stream("sp", me, late, lambda i: obuf.at[i, pl.ds(ocut, 2 * cw - ocut)], o_ss, o_rs, 0, started)
    op = Stream("sp", me, early, lambda i: obuf.at[i, pl.ds(0, ocut)], o_ss, o_rs, S, started)
    aa = Stream("tp", tp, [1 << k for k in reversed(range(T.bit_length() - 1))], lambda i: abuf.at[i], a_ss, a_rs, 0, started)
    masks = sorted(range(1, S), key=lambda m: (bin(m).count("1"), m))
    even = [m for m in masks if m % 2 == 0]
    odd = [m for m in masks if m % 2 == 1]
    wp.push(0)
    wq.push(0)
    sq_.push(0)
    aa.push(0)
    wp.got(1)
    aa.got(2)
    wq.got(even[0])
    sq_.got(even[0])
    for mask in range(1, T):
        if mask != 2:
            aa.got(mask)
    per = da // kd
    rt = 64

    def norm_rows(i, _):
        r = pl.ds(pl.multiple_of(i * rt, rt), rt)
        parts = [abuf[t, r, :].astype(F32) for t in range(T)]
        tot = sum(jnp.sum(p * p, axis=-1, keepdims=True) for p in parts)
        rs = lax.rsqrt(tot / (da * T) + EPSILON)
        for t in range(T):
            g = abuf[t, n : n + 1, :].astype(F32)
            v = (parts[t] * rs * g).astype(BF)
            for j in range(per):
                nbuf[t * per + j, r, :] = v[:, j * kd : (j + 1) * kd]
        return 0

    lax.fori_loop(0, n // rt, norm_rows, 0)
    mt = 256

    def add_chunk(i, first):
        for r0 in range(0, n, mt):
            x = nbuf[i, r0 : r0 + mt, :]
            d = jnp.dot(x, wbuf[i], preferred_element_type=F32)
            if first:
                acc[r0 : r0 + mt, :] = d
            else:
                acc[r0 : r0 + mt, :] += d
        d = bt(sbuf[i], nbuf[i])
        if first:
            sacc[...] = d
        else:
            sacc[...] += d

    add_chunk(me, True)
    for k, mask in enumerate(even):
        if k:
            wq.got(mask)
            sq_.got(mask)
        if k == 1:
            for m in early_first(S):
                wp.got(m)
        if k == len(even) - 1:
            op.push(0)
            oq.push(0)
    rest = [m for m in masks if m != 1 and m not in early_first(S)]
    for mask in even:
        if mask in rest:
            wp.got(mask)
        add_chunk(flip(me, mask), False)
    for mask in odd:
        if mask in rest:
            wp.got(mask)
        wq.got(mask)
        sq_.got(mask)
        add_chunk(flip(me, mask), False)

    raw0 = 16
    ccol = ncol - cw
    hsend[:, 0:cw] = acc[n - raw0 :, 0:cw].astype(BF)
    hsend[:, cw:] = acc[n - raw0 :, 2 * cw :].astype(BF)

    def halo():
        return remote(hsend, hrecv, h_ss, h_rs, sp=lax.rem(me + 1, S))

    @pl.when(me < S - 1)
    def _():
        halo().start()

    ext[raw0:, 0:cw] = acc[:, 0:cw].astype(BF).astype(F32)
    ext[raw0:, cw:] = acc[:, 2 * cw :].astype(BF).astype(F32)

    def column(row):
        return bt(pick, jnp.broadcast_to(row[...], (8, heads)), precision=HIGH)[:, 0:1]

    step = sacc[...] + column(bias)
    step = jnp.maximum(step, 0.0) + jnp.log1p(jnp.exp(-jnp.abs(step)))
    ld = -jnp.exp(column(dlog)) * step + jnp.dot(pick, extra_t[...], precision=HIGH, preferred_element_type=F32)
    r_i = lax.broadcasted_iota(jnp.int32, (blk, blk), 0)
    c_i = lax.broadcasted_iota(jnp.int32, (blk, blk), 1)
    upper = jnp.where(r_i <= c_i, 1.0, 0.0).astype(F32)
    eye = jnp.where(r_i == c_i, 1.0, 0.0).astype(F32)
    lower = r_i >= c_i
    expand = jnp.where(
        lax.broadcasted_iota(jnp.int32, (hp, cw), 1) // hd == lax.broadcasted_iota(jnp.int32, (hp, cw), 0), 1.0, 0.0
    ).astype(F32)
    skips = jnp.dot(
        jnp.broadcast_to(skip[...], (8, heads)), expand[0:heads, :], precision=HIGH, preferred_element_type=F32
    )[0:1, :]
    eye_st = jnp.where(
        lax.broadcasted_iota(jnp.int32, (st, st), 0) == lax.broadcasted_iota(jnp.int32, (st, st), 1), 1.0, 0.0
    ).astype(BF)
    cum_rs, cum_cs, st_rs, wexps = [], [], [], []
    for b in range(blocks):
        cols = slice(b * blk, (b + 1) * blk)
        cum_r = jnp.dot(ld[:, cols], upper, precision=HIGH, preferred_element_type=F32)
        st_r = step[:, cols]
        turned = bt(eye, jnp.concatenate([cum_r, st_r], axis=0), precision=HIGH)
        cum_c = turned[:, 0:hp]
        w_c = jnp.exp(cum_c[blk - 1 : blk, :] - cum_c) * turned[:, hp:]
        both = jnp.dot(
            jnp.concatenate([w_c, jnp.exp(cum_c)], axis=0), expand, precision=HIGH, preferred_element_type=F32
        )
        expd[cols, :] = both[blk:, :]
        wexps.append(both[:blk, :])
        cum_rs.append(cum_r)
        cum_cs.append(cum_c)
        st_rs.append(st_r)

    @pl.when(me > 0)
    def _():
        halo().wait_recv()
        ext[0:raw0, :] = hrecv[...].astype(F32)

    @pl.when(me == 0)
    def _():
        ext[0:raw0, :] = jnp.zeros((raw0, ext.shape[1]), F32)

    width = taps_v.shape[0]
    for b in range(blocks):
        for taps, lo, hi in ((taps_v, 0, cw), (taps_k, cw, cw + st), (taps_r, cw + st, cw + 2 * st)):
            total = jnp.zeros((blk, hi - lo), F32)
            for k in range(width):
                o = b * blk + raw0 - (width - 1) + k
                total = total + taps[k : k + 1, :] * ext[o : o + blk, cw + lo : cw + hi]
            conv[b * blk : (b + 1) * blk, lo:hi] = (total * jax.nn.sigmoid(total)).astype(BF)

    run = jnp.zeros((st, cw), F32)
    dec = jnp.ones((1, cw), F32)
    pres, offs = [], []
    for b in range(blocks):
        rows = slice(b * blk, (b + 1) * blk)
        key_t = bt(eye_st, conv[rows, cw : cw + st]).astype(BF)
        sv = conv[rows, 0:cw].astype(F32) * wexps[b]
        top, low = halves(sv)
        new = jnp.dot(key_t, top, preferred_element_type=F32) + jnp.dot(key_t, low, preferred_element_type=F32)
        bd = expd[(b + 1) * blk - 1 : (b + 1) * blk, :]
        pres.append(run)
        offs.append(dec)
        run = run * bd + new
        dec = dec * bd

    in_s = jnp.zeros((st, cw), F32)
    in_d = jnp.ones((1, cw), F32)
    rounds = [1 << k for k in range(S.bit_length() - 1)]

    def inner(b):
        rows = slice(b * blk, (b + 1) * blk)
        g = bt(conv[rows, cw + st :], conv[rows, cw : cw + st])
        for h in range(cw // hd):
            gap = jnp.where(lower, cum_cs[b][:, h : h + 1] - cum_rs[b][h : h + 1, :], -jnp.inf)
            wm = g * jnp.exp(gap) * st_rs[b][h : h + 1, :]
            top, low = halves(wm)
            v = conv[rows, h * hd : (h + 1) * hd]
            scan[rows, h * hd : (h + 1) * hd] = jnp.dot(top, v, preferred_element_type=F32) + jnp.dot(
                low, v, preferred_element_type=F32
            )

    window = lax.shift_left(jnp.int32(2), tp)
    back = (
        lax.broadcasted_iota(jnp.int32, (blk, blk + raw0), 0)
        + raw0
        - lax.broadcasted_iota(jnp.int32, (blk, blk + raw0), 1)
    )
    band = jnp.where((back >= 0) & (back < window), 1.0, 0.0).astype(BF)

    def pool(b):
        rows = slice(b * blk, (b + 1) * blk)
        sums = jnp.dot(band, ext[b * blk : (b + 1) * blk + raw0, 0:cw].astype(BF), preferred_element_type=F32)
        pos = (me * n + b * blk + lax.broadcasted_iota(jnp.int32, (blk, cw), 0)).astype(F32)
        counts = jnp.minimum(pos + 1.0, window.astype(F32))
        pooled = (sums / counts - ext[b * blk + raw0 : (b + 1) * blk + raw0, 0:cw]).astype(BF)
        brow[rows, 0:cw] = (jnp.dot(pooled, mix[0], preferred_element_type=F32) * scale[...]).astype(BF)

    work = [functools.partial(inner, b) for b in range(blocks)] + [functools.partial(pool, b) for b in range(blocks)]
    share = -(-len(work) // len(rounds))
    o_left = [(op, 1), (oq, even[0])] + [(op, m) for m in early_first(S)] + [(oq, m) for m in even[1:]]
    o_step = -(-len(o_left) // len(rounds))
    o_rest = [(op, m) for m in masks if (op, m) not in o_left] + [(oq, m) for m in odd]

    def take_o(count):
        for stream, mask in o_left[:count]:
            stream.got(mask)
        del o_left[:count]

    for r, bit in enumerate(rounds):
        xs[r, 0:st, :] = run
        xs[r, st:, :] = jnp.broadcast_to(dec, (xs.shape[1] - st, cw))
        send(xs.at[r], xr.at[r], x_ss.at[r], x_rs.at[r], sp=flip(me, bit))
        for f in work[r * share : (r + 1) * share]:
            f()
        take_o(o_step)
        remote(xs.at[r], xr.at[r], x_ss.at[r], x_rs.at[r], sp=flip(me, bit)).wait_recv()
        other, odec = xr[r, 0:st, :], xr[r, st : st + 1, :]
        later = lax.rem(lax.div(me, bit), 2) == 1
        in_s = jnp.where(later, other * in_d + in_s, in_s)
        in_d = jnp.where(later, odec * in_d, in_d)
        run = jnp.where(later, other * dec + run, run * odec + other)
        dec = dec * odec

    for b in range(blocks):
        rows = slice(b * blk, (b + 1) * blk)
        top, low = halves(pres[b] + offs[b] * in_s)
        rd = conv[rows, cw + st :]
        carried = jnp.dot(rd, top, preferred_element_type=F32) + jnp.dot(rd, low, preferred_element_type=F32)
        y = scan[rows, :] + carried * expd[rows, :] + skips * conv[rows, 0:cw].astype(F32)
        gt = acc[rows, cw : 2 * cw].astype(BF).astype(F32)
        gated = y * (gt * jax.nn.sigmoid(gt))
        ssend[:, rows] = bt(jnp.ones((8, cw), F32), gated * gated, precision=HIGH)
        brow[rows, cw:] = (gated * sgain[...]).astype(BF)
    for k in range(1, T):
        send(ssend, srecv.at[k - 1], q_ss.at[k - 1], q_rs.at[k - 1], tp=flip(tp, k))
    take_o(len(o_left))
    for stream, mask in o_rest:
        stream.got(mask)
    for k in range(1, T):
        remote(ssend, srecv.at[k - 1], q_ss.at[k - 1], q_rs.at[k - 1], tp=flip(tp, k)).wait_recv()
    sq = ssend[...]
    for k in range(1, T):
        sq = sq + srecv[k - 1]
    rs_row = lax.rsqrt(sq / (cw * T) + EPSILON)
    rs_cols = [bt(eye, rs_row[:, b * blk : (b + 1) * blk], precision=HIGH)[:, 0:1] for b in range(blocks)]
    wide = S // T
    oc = obuf.shape[2]
    parts = 4
    pr = n // parts

    def product(t, part, store):
        rows = slice(part * pr, (part + 1) * pr)
        rs = jnp.concatenate(rs_cols[part * blocks // parts : (part + 1) * blocks // parts], axis=0)
        for j in range(wide):
            i = t * wide + j
            p = jnp.dot(brow[rows, 0:cw], obuf[i, 0:cw, :], preferred_element_type=F32)
            p = p + rs * jnp.dot(brow[rows, cw:], obuf[i, cw:, :], preferred_element_type=F32)
            store(rows, slice(j * oc, (j + 1) * oc), p)

    def into(ref, *lead):
        def store(rows, cols, p):
            ref[lead + (rows, cols)] = p.astype(ref.dtype)
        return store

    near = flip(tp, 1)

    def near_copy(k, part):
        rows = pl.ds(part * pr, pr)
        i = k * parts + part
        return remote(psend.at[k, rows], precv.at[k, rows], p_ss.at[i], p_rs.at[i], tp=near)

    def far_copy(part):
        rows = pl.ds(part * pr, pr)
        return remote(qsend.at[rows], qrecv.at[rows], r_ss.at[part], r_rs.at[part], tp=flip(tp, 2))

    for part in range(parts):
        product(flip(tp, 3), part, into(psend, 0))
        near_copy(0, part).start()
    for part in range(parts):
        rows = slice(part * pr, (part + 1) * pr)
        product(flip(tp, 2), part, into(pown))
        near_copy(0, part).wait_recv()
        qsend[rows, :] = (pown[rows, :] + precv[0, rows, :]).astype(BF)
        far_copy(part).start()
    for part in range(parts):
        product(near, part, into(psend, 1))
        near_copy(1, part).start()
    for part in range(parts):
        product(tp, part, into(pown))
    for part in range(parts):
        rows = slice(part * pr, (part + 1) * pr)
        near_copy(1, part).wait_recv()
        far_copy(part).wait_recv()
        out[rows, :] = (pown[rows, :] + precv[1, rows, :] + qrecv[rows, :].astype(F32)).astype(out.dtype)

    for c in started:
        c.wait_send()
    for part in range(parts):
        near_copy(0, part).wait_send()
        near_copy(1, part).wait_send()
        far_copy(part).wait_send()

    @pl.when(me < S - 1)
    def _():
        halo().wait_send()


def fits(S, T, shapes):
    n, da = shapes[0]
    kd, cw = shapes[2]
    st = shapes[5][1]
    oc = shapes[18][1]
    heads = shapes[7][1]
    return (
        T == 4 == POOL_GROUPS and S >= T and S & (S - 1) == 0 and S <= 16 and st == SSM_STATE
        and cw == heads * SSM_STATE and n % (4 * SCAN_BLOCK) == 0
        and -(-kd // 96) * 2 * cw % kd == 0 and oc % 128 == 0 and kd % 128 == 0 and da % kd == 0
        and n % (2 * SCAN_BLOCK) == 0 and cw % 128 == 0 and oc * S == da * T
    )


def fused(
    S, T, activations, norm_gain, pool_weight, gate_weight, value_weight, key_weight, read_weight,
    step_weight, pool_mix, pool_scale, taps_value, taps_key, taps_read, step_bias, decay_log,
    decay_extra, skip_scale, state_gain, out_pool_weight, out_state_weight,
):
    n, da = activations.shape
    kd, cw = pool_weight.shape
    st = key_weight.shape[1]
    heads = step_weight.shape[1]
    oc = out_pool_weight.shape[1]
    hp = 16
    args = (
        activations, norm_gain[None, :], pool_weight, gate_weight, value_weight, key_weight.T, read_weight.T,
        step_weight.T, pool_mix, pool_scale[None, :], taps_value, taps_key, taps_read, step_bias[None, :], decay_log[None, :],
        decay_extra.T, skip_scale[None, :], state_gain[None, :],
        out_pool_weight, out_state_weight,
    )
    ncol = 3 * cw + 2 * st
    ccol = ncol - cw
    V = pltpu.VMEM
    D = pltpu.SemaphoreType.DMA
    R = S.bit_length() - 1
    scratch = [
        V((S, kd, ncol), BF), V((S, hp, kd), BF), V((S, 2 * cw, oc), BF), V((T, n + 16, da), BF),
        V((S, n, kd), BF), V((n, ncol), F32), V((hp, n), F32), V((n + 16, ccol), F32),
        V((n, cw + 2 * st), BF), V((16, ccol), BF), V((16, ccol), BF), V((n, cw), F32),
        V((R, st + 8, cw), F32), V((R, st + 8, cw), F32), V((8, n), F32), V((T - 1, 8, n), F32),
        V((n, 2 * cw), BF), V((2, n, da), F32), V((2, n, da), F32), V((n, da), F32),
        V((n, da), BF), V((n, da), BF), V((n, cw), F32),
        D((2 * S,)), D((2 * S,)), D((S,)), D((S,)), D((2 * S,)), D((2 * S,)), D((T,)), D((T,)), D, D,
        D((R,)), D((R,)), D((T,)), D((T,)), D((8,)), D((8,)), D((4,)), D((4,)),
    ]
    return pl.pallas_call(
        functools.partial(mixer_kernel, S, T),
        out_shape=jax.ShapeDtypeStruct((n, da), BF),
        in_specs=[pl.BlockSpec(memory_space=pltpu.VMEM)] * len(args),
        out_specs=pl.BlockSpec(memory_space=pltpu.VMEM),
        scratch_shapes=scratch,
        compiler_params=pltpu.CompilerParams(
            collective_id=0, has_side_effects=True, vmem_limit_bytes=60 * 1024 * 1024
        ),
    )(*args)


def solution(mesh):
    placed = (
        P("sp", "tp"),
        P("tp"),
        P("sp", "tp"),
        P("sp", "tp"),
        P("sp", "tp"),
        P("sp", "tp"),
        P("sp", "tp"),
        P("sp", "tp"),
        P("tp", None, None),
        P("tp"),
        P(None, "tp"),
        P(None, "tp"),
        P(None, "tp"),
        P("tp"),
        P("tp"),
        P("sp", "tp"),
        P("tp"),
        P("tp"),
        P("tp", "sp"),
        P("tp", "sp"),
    )
    S, T = mesh.shape["sp"], mesh.shape["tp"]

    def chosen(*args):
        if fits(S, T, [a.shape for a in args]):
            return fused(S, T, *args)
        return local(*args)

    return jax.shard_map(
        chosen, mesh=mesh, in_specs=placed, out_specs=P("sp", "tp"), check_vma=False
    )
```

profile of v0, /device:TPU:1, one launch (start us, length us, event | category | flops | bytes accessed | tf_op | source)
XLA Modules:
  0.0 101.5 jit_solution(14737168095461935028)
XLA Ops:
  0.0 0.0 copy-start
  0.0 0.7 copy-done
  0.7 0.6 broadcast_in_dim.18.gain
  1.3 98.4 %shard_map.190 = bf16[512,512]{1,0:T(8,128)(2,1)} custom-call(bf16[512,512]{1,0:T(8,128)(2,1)} %act.1, bf16[1,512]{1,0:T(2,128)(2,1)} %broadcast_in_dim.18.gain, bf16[256,256]{1,0:T(8,128)(2,1)} %pool_w.1, bf16[256,256]{1,0:T(8,128)(2,1)} %gate_w.1, bf16[256,256]{1,0:T(8,128)(2,1)} %value_w.1, bf16[64,256]{1,0:T(8,128)(2,1)} %bitcast.9, ...), custom_call_target="tpu_custom_call" | custom-call | tf_op jit(solution)/shard_map/pallas_call | solution.py:679
  99.6 1.9 %copy.22 = bf16[512,512]{1,0:T(8,128)(2,1)} copy(bf16[512,512]{1,0:T(8,128)(2,1)} %shard_map.190) | data formatting | bytes 1048576
Async XLA Ops:
  0.0 0.7 copy-start
where the time goes:
time: 102 us
  Pallas kernels  98.4 us (96%)
  local copies, waits for them, and re-layouts  3.13 us (3%)
    pallas_call x1, Pallas kernels, fused(): pl.pallas_call(functools.partial(mixer_kernel, S, T), out_shape=jax.Shape...  98.4 us
    unnamed x3, local copies, waits for them, and re-layouts  2.55 us

commit v1 on v0

--- a/solution.py
+++ b/solution.py
@@ -220,43 +220,6 @@
     return index
 
 
-class Stream:
-    def __init__(self, axis, place, bits, refs, send_sems, recv_sems, base, started):
-        self.axis, self.place, self.bits, self.refs = axis, place, bits, refs
-        self.send_sems, self.recv_sems, self.base, self.started = send_sems, recv_sems, base, started
-
-    def via(self, mask):
-        return [bit for bit in self.bits if mask & bit][-1]
-
-    def copy(self, mask, bit):
-        ref = self.refs(flip(self.place, mask))
-        slot = self.base + (mask | bit)
-        return pltpu.make_async_remote_copy(
-            src_ref=ref, dst_ref=ref, send_sem=self.send_sems.at[slot], recv_sem=self.recv_sems.at[slot],
-            device_id={self.axis: flip(self.place, bit)}, device_id_type=MESH,
-        )
-
-    def push(self, mask):
-        onward = self.bits if mask == 0 else self.bits[self.bits.index(self.via(mask)) + 1 :]
-        for bit in sorted(onward):
-            c = self.copy(mask, bit)
-            c.start()
-            self.started.append(c)
-
-    def got(self, mask):
-        ref = self.refs(flip(self.place, mask))
-        slot = self.base + mask
-        pltpu.make_async_remote_copy(
-            src_ref=ref, dst_ref=ref, send_sem=self.send_sems.at[slot], recv_sem=self.recv_sems.at[slot],
-            device_id={self.axis: flip(self.place, self.via(mask))}, device_id_type=MESH,
-        ).wait_recv()
-        self.push(mask)
-
-
-def early_first(size):
-    return [m for m in range(2, size) if m // 2 & (m // 2 - 1) == 0 and m > 3]
-
-
 def bt(a, b, **kw):
     return lax.dot_general(a, b, (((1,), (1,)), ((), ())), preferred_element_type=F32, **kw)
 
@@ -271,83 +234,256 @@
     act, gain, pool_w, gate_w, value_w, key_w, read_w, step_t, mix, scale, taps_v, taps_k, taps_r,
     bias, dlog, extra_t, skip, sgain, opool, ostate,
     out,
-    wbuf, sbuf, obuf, abuf, nbuf, acc, sacc, ext, conv, hsend, hrecv, scan, xs, xr, ssend, srecv,
-    brow, psend, precv, pown, qsend, qrecv, expd,
-    w_ss, w_rs, s_ss, s_rs, o_ss, o_rs, a_ss, a_rs, h_ss, h_rs, x_ss, x_rs, q_ss, q_rs, p_ss, p_rs, r_ss, r_rs,
+    vbuf, gbuf, obuf, abuf, mixb, par, nbuf, extv, extp, gateb, conv, hvs, hvr, hps, hpr, scan, xs, xr,
+    sq_buf, pbuf, sbuf, expd,
+    b_ss, b_rs, o_ss, o_rs, a_ss, a_rs, t_ss, t_rs, h_ss, h_rs, x_ss, x_rs, q_ss, q_rs, p_ss, p_rs,
 ):
     n, da = act.shape
-    kd = pool_w.shape[0]
-    cw = pool_w.shape[1]
+    kd, cw = pool_w.shape
     st = key_w.shape[0]
-    ncol = wbuf.shape[2]
+    heads = step_t.shape[0]
+    hp = vbuf.shape[1] - kd
+    vc = cw + 2 * st
+    oc = opool.shape[1]
     blk = SCAN_BLOCK
     blocks = n // blk
     hd = SSM_STATE
-    me = lax.axis_index("sp")
-    tp = lax.axis_index("tp")
-    wbuf[me, :, 0:cw] = pool_w[...]
-    wbuf[me, :, cw : 2 * cw] = gate_w[...]
-    wbuf[me, :, 2 * cw : 3 * cw] = value_w[...]
+    Z = S // 2
+    sp, tq = lax.axis_index("sp"), lax.axis_index("tp")
+    z, y = lax.div(sp, 2), lax.rem(sp, 2)
+    x, c = lax.div(tq, 2), lax.rem(tq, 2)
+    me, tp = 2 * z + c, 2 * x + y
+    off = lax.rem(y + c, 2)
+    moved, kept = off == 1, off == 0
+    slot = me + off * (S - me)
+    aslot = tq + off * (T - tq)
+    pslot = tp + off * (T - tp)
+    hub = tq == z
+    oslot = jnp.where(hub, y * T + tq, 2 * T)
+
+    def dev(z_=z, y_=y, x_=x, c_=c):
+        return {"sp": 2 * z_ + y_, "tp": 2 * x_ + c_}
+
+    def copy(src, dst, ss, rs, **to):
+        return pltpu.make_async_remote_copy(
+            src_ref=src, dst_ref=dst, send_sem=ss, recv_sem=rs, device_id=dev(**to), device_id_type=MESH
+        )
+
     eye_kd = jnp.where(
         lax.broadcasted_iota(jnp.int32, (kd, kd), 0) == lax.broadcasted_iota(jnp.int32, (kd, kd), 1), 1.0, 0.0
     ).astype(BF)
-    wbuf[me, :, 3 * cw :] = bt(eye_kd, jnp.concatenate([key_w[...], read_w[...]], axis=0)).astype(BF)
-    hp = sbuf.shape[1]
-    heads = step_t.shape[0]
     pick = jnp.where(
         lax.broadcasted_iota(jnp.int32, (hp, heads), 0) == lax.broadcasted_iota(jnp.int32, (hp, heads), 1), 1.0, 0.0
     ).astype(F32)
-    sbuf[me] = jnp.dot(pick.astype(BF), step_t[...], preferred_element_type=F32).astype(BF)
-    abuf[tp, 0:n, :] = act[...]
-    abuf[tp, n : n + 16, :] = jnp.broadcast_to(gain[...].astype(F32), (16, da)).astype(BF)
+    vbuf[slot, 0:kd, 0:cw] = value_w[...]
+    vbuf[slot, 0:kd, cw:] = bt(eye_kd, jnp.concatenate([key_w[...], read_w[...]], axis=0)).astype(BF)
+    vbuf[slot, kd:, :] = jnp.zeros((hp, vc), BF)
+    vbuf[slot, kd:, 0:kd] = jnp.dot(pick.astype(BF), step_t[...], preferred_element_type=F32).astype(BF)
+    abuf[aslot, 0:n, :] = act[...]
+    abuf[aslot, n : n + 16, :] = jnp.broadcast_to(gain[...].astype(F32), (16, da)).astype(BF)
 
     barrier = pltpu.get_barrier_semaphore()
-    for k in range(1, S):
-        pl.semaphore_signal(barrier, inc=1, device_id={"sp": lax.rem(me + k, S)}, device_id_type=MESH)
-    for k in range(1, T):
-        pl.semaphore_signal(barrier, inc=1, device_id={"tp": lax.rem(tp + k, T)}, device_id_type=MESH)
-    obuf[me, 0:cw, :] = opool[...]
-    obuf[me, cw:, :] = ostate[...]
-    pl.semaphore_wait(barrier, S - 1 + T - 1)
-
-    started = []
-
-    def remote(src, dst, ss, rs, **peer):
-        c = pltpu.make_async_remote_copy(
-            src_ref=src, dst_ref=dst, send_sem=ss, recv_sem=rs, device_id=peer, device_id_type=MESH
+
+    def greet(**to):
+        pl.semaphore_signal(barrier, inc=1, device_id=dev(**to), device_id_type=MESH)
+
+    for k in range(1, 8):
+        greet(
+            y_=1 - y if k & 4 else y, x_=1 - x if k & 2 else x, c_=1 - c if k & 1 else c,
         )
-        return c
-
-    def send(*a, **k):
-        c = remote(*a, **k)
-        c.start()
-        started.append(c)
-
-    far = [1 << k for k in reversed(range(1, S.bit_length() - 1))]
-    late = far + [1]
-    early = [1] + far
-    cut = -(-kd // 96) * 16
-    ocut = cut * 2 * cw // kd
-    wq = Stream("sp", me, late, lambda i: wbuf.at[i, pl.ds(cut, kd - cut)], w_ss, w_rs, 0, started)
-    wp = Stream("sp", me, early, lambda i: wbuf.at[i, pl.ds(0, cut)], w_ss, w_rs, S, started)
-    sq_ = Stream("sp", me, late, lambda i: sbuf.at[i], s_ss, s_rs, 0, started)
-    oq = Stream("sp", me, late, lambda i: obuf.at[i, pl.ds(ocut, 2 * cw - ocut)], o_ss, o_rs, 0, started)
-    op = Stream("sp", me, early, lambda i: obuf.at[i, pl.ds(0, ocut)], o_ss, o_rs, S, started)
-    aa = Stream("tp", tp, [1 << k for k in reversed(range(T.bit_length() - 1))], lambda i: abuf.at[i], a_ss, a_rs, 0, started)
-    masks = sorted(range(1, S), key=lambda m: (bin(m).count("1"), m))
-    even = [m for m in masks if m % 2 == 0]
-    odd = [m for m in masks if m % 2 == 1]
-    wp.push(0)
-    wq.push(0)
-    sq_.push(0)
-    aa.push(0)
-    wp.got(1)
-    aa.got(2)
-    wq.got(even[0])
-    sq_.got(even[0])
-    for mask in range(1, T):
-        if mask != 2:
-            aa.got(mask)
+    for k in range(1, Z):
+        greet(z_=lax.rem(z + k, Z))
+        greet(z_=lax.rem(z + k, Z), c_=1 - c)
+    gbuf[slot, :, 0:cw] = pool_w[...]
+    gbuf[slot, :, cw:] = gate_w[...]
+    obuf[oslot, 0:cw, :] = opool[...]
+    obuf[oslot, cw:, :] = ostate[...]
+    mixb[off] = mix[0]
+    par[off] = jnp.zeros(par.shape[1:], F32)
+    par[off, 0:heads, :] = extra_t[...]
+    par[off, 16:17, 0:cw] = scale[...]
+    par[off, 16:17, cw : 2 * cw] = sgain[...]
+    par[off, 17:18, 0:heads] = bias[...]
+    par[off, 18:19, 0:heads] = dlog[...]
+    par[off, 19:20, 0:heads] = skip[...]
+    width = taps_v.shape[0]
+    par[off, 24 : 24 + width, 0:cw] = taps_v[...]
+    par[off, 24 : 24 + width, cw : cw + st] = taps_k[...]
+    par[off, 24 : 24 + width, cw + st : vc] = taps_r[...]
+    pl.semaphore_wait(barrier, 7 + 2 * (Z - 1))
+
+    streams = (vbuf, gbuf)
+
+    def bcopy(k, i, way):
+        to = ({"c_": 1 - c}, {"z_": z + 1}, {"z_": z - 1})[way]
+        ref = streams[k].at[i]
+        return copy(ref, ref, b_ss.at[(k * S + i) * 3 + way], b_rs.at[k * S + i], **to)
+
+    def arrived(k, i):
+        bcopy(k, i, 0).wait_recv()
+
+    def source(k, do):
+        @pl.when(z < Z - 1)
+        def _():
+            do(bcopy(k, me, 1))
+
+        @pl.when(z > 0)
+        def _():
+            do(bcopy(k, me, 2))
+
+        do(bcopy(k, me, 0))
+
+    def start(d):
+        d.start()
+
+    def done(d):
+        d.wait_send()
+
+    def pump(k, d, do, wait=True):
+        @pl.when(z >= d)
+        def _():
+            i = 2 * (z - d) + c
+            if wait:
+                arrived(k, i)
+
+            @pl.when(z < Z - 1)
+            def _():
+                do(bcopy(k, i, 1))
+
+            do(bcopy(k, i, 0))
+
+        @pl.when(z + d < Z)
+        def _():
+            i = 2 * (z + d) + c
+            if wait:
+                arrived(k, i)
+
+            @pl.when(z > 0)
+            def _():
+                do(bcopy(k, i, 2))
+
+            do(bcopy(k, i, 0))
+
+    def partners(k):
+        for p in range(Z):
+            arrived(k, 2 * p + 1 - c)
+
+    def swap(i):
+        src, dst, rs = (
+            (vbuf.at[S], vbuf.at[sp], b_rs.at[sp]),
+            (par.at[1], par.at[0], t_rs.at[0]),
+            (gbuf.at[S], gbuf.at[sp], b_rs.at[S + sp]),
+            (mixb.at[1], mixb.at[0], t_rs.at[1]),
+        )[i]
+        return copy(src, dst, t_ss.at[i], rs, y_=c, c_=y)
+
+    def acopy(way):
+        to = ({"c_": y}, {"x_": 1 - x, "c_": y}, {"y_": 1 - y, "c_": y})[way]
+        return copy(abuf.at[aslot], abuf.at[tq], a_ss.at[way], a_rs.at[tq], **to)
+
+    def aforward(f):
+        t = 2 * x + f
+        return copy(abuf.at[t], abuf.at[t], a_ss.at[3 + f], a_rs.at[t], x_=1 - x)
+
+    def agot(t):
+        copy(abuf.at[t], abuf.at[t], a_ss.at[0], a_rs.at[t], x_=1 - x).wait_recv()
+
+    def ohub():
+        return copy(
+            obuf.at[2 * T], obuf.at[y * T + tq], o_ss.at[0], o_rs.at[y * T + tq], x_=lax.div(z, 2), c_=lax.rem(z, 2)
+        )
+
+    def ocopy(q, way):
+        to = ({"y_": 1 - y}, {"z_": z + 1}, {"z_": z - 1})[way]
+        ref = obuf.at[y * T + q]
+        return copy(ref, ref, o_ss.at[1 + q * 3 + way], o_rs.at[y * T + q], **to)
+
+    def omoves(q, do):
+        @pl.when((z >= tq) & (z < Z - 1))
+        def _():
+            do(ocopy(q, 1))
+
+        @pl.when((z <= tq) & (z > 0))
+        def _():
+            do(ocopy(q, 2))
+
+        do(ocopy(q, 0))
+
+    def oslice(tau):
+        for q in range(T):
+            d = tau - q
+            if d == 0:
+                @pl.when(hub)
+                def _():
+                    @pl.when(tq != q)
+                    def _():
+                        ocopy(q, 0).wait_recv()
+
+                    omoves(q, start)
+            elif 0 < d < Z:
+                @pl.when((z == tq + d) | (z == tq - d))
+                def _():
+                    ocopy(q, 0).wait_recv()
+                    omoves(q, start)
+
+    @pl.when(moved)
+    def _():
+        swap(0).start()
+
+    acopy(1).start()
+    acopy(2).start()
+
+    @pl.when(moved)
+    def _():
+        acopy(0).start()
+        for i in range(1, 4):
+            swap(i).start()
+
+    @pl.when(jnp.logical_not(hub))
+    def _():
+        ohub().start()
+
+    @pl.when(moved)
+    def _():
+        arrived(0, me)
+
+    source(0, start)
+
+    @pl.when(kept)
+    def _():
+        source(1, start)
+
+    @pl.when(moved)
+    def _():
+        agot(2 * x + c)
+        aforward(c).start()
+
+    pump(0, 1, start)
+
+    @pl.when(moved)
+    def _():
+        agot(2 * x + 1 - c)
+        aforward(1 - c).start()
+
+    pump(0, 2, start)
+
+    @pl.when(moved)
+    def _():
+        arrived(1, me)
+        source(1, start)
+
+    oslice(0)
+    pump(1, 1, start)
+    pump(0, 3, start)
+    partners(0)
+
+    @pl.when(kept)
+    def _():
+        agot(2 * x + 1 - c)
+
+    agot(2 * (1 - x))
+    agot(2 * (1 - x) + 1)
+
     per = da // kd
     rt = 64
 
@@ -365,65 +501,41 @@
 
     lax.fori_loop(0, n // rt, norm_rows, 0)
     mt = 256
-
-    def add_chunk(i, first):
-        for r0 in range(0, n, mt):
-            x = nbuf[i, r0 : r0 + mt, :]
-            d = jnp.dot(x, wbuf[i], preferred_element_type=F32)
-            if first:
-                acc[r0 : r0 + mt, :] = d
-            else:
-                acc[r0 : r0 + mt, :] += d
-        d = bt(sbuf[i], nbuf[i])
-        if first:
-            sacc[...] = d
-        else:
-            sacc[...] += d
-
-    add_chunk(me, True)
-    for k, mask in enumerate(even):
-        if k:
-            wq.got(mask)
-            sq_.got(mask)
-        if k == 1:
-            for m in early_first(S):
-                wp.got(m)
-        if k == len(even) - 1:
-            op.push(0)
-            oq.push(0)
-    rest = [m for m in masks if m != 1 and m not in early_first(S)]
-    for mask in even:
-        if mask in rest:
-            wp.got(mask)
-        add_chunk(flip(me, mask), False)
-    for mask in odd:
-        if mask in rest:
-            wp.got(mask)
-        wq.got(mask)
-        sq_.got(mask)
-        add_chunk(flip(me, mask), False)
-
     raw0 = 16
-    ccol = ncol - cw
-    hsend[:, 0:cw] = acc[n - raw0 :, 0:cw].astype(BF)
-    hsend[:, cw:] = acc[n - raw0 :, 2 * cw :].astype(BF)
-
-    def halo():
-        return remote(hsend, hrecv, h_ss, h_rs, sp=lax.rem(me + 1, S))
+
+    for r0 in range(0, n, mt):
+        d = jnp.dot(nbuf[0, r0 : r0 + mt, :], vbuf[0, 0:kd, :], preferred_element_type=F32)
+        for i in range(1, S):
+            d = d + jnp.dot(nbuf[i, r0 : r0 + mt, :], vbuf[i, 0:kd, :], preferred_element_type=F32)
+        low = d.astype(BF)
+        extv[raw0 + r0 : raw0 + r0 + mt, :] = low.astype(F32)
+        if r0 + mt == n:
+            hvs[...] = low[mt - raw0 :, :]
+
+    def halo(src, dst, i):
+        return copy(src, dst, h_ss.at[i], h_rs.at[i], z_=z + c, c_=1 - c)
 
     @pl.when(me < S - 1)
     def _():
-        halo().start()
-
-    ext[raw0:, 0:cw] = acc[:, 0:cw].astype(BF).astype(F32)
-    ext[raw0:, cw:] = acc[:, 2 * cw :].astype(BF).astype(F32)
+        halo(hvs, hvr, 0).start()
+
+    sacc = bt(vbuf[0, kd:, 0:kd], nbuf[0])
+    for i in range(1, S):
+        sacc = sacc + bt(vbuf[i, kd:, 0:kd], nbuf[i])
+    oslice(1)
+    pump(1, 2, start)
+
+    @pl.when(moved)
+    def _():
+        swap(1).wait_recv()
+        swap(3).wait_recv()
 
     def column(row):
-        return bt(pick, jnp.broadcast_to(row[...], (8, heads)), precision=HIGH)[:, 0:1]
-
-    step = sacc[...] + column(bias)
+        return bt(pick, jnp.broadcast_to(row, (8, heads)), precision=HIGH)[:, 0:1]
+
+    step = sacc + column(par[0, 17:18, 0:heads])
     step = jnp.maximum(step, 0.0) + jnp.log1p(jnp.exp(-jnp.abs(step)))
-    ld = -jnp.exp(column(dlog)) * step + jnp.dot(pick, extra_t[...], precision=HIGH, preferred_element_type=F32)
+    ld = -jnp.exp(column(par[0, 18:19, 0:heads])) * step + par[0, 0:hp, :]
     r_i = lax.broadcasted_iota(jnp.int32, (blk, blk), 0)
     c_i = lax.broadcasted_iota(jnp.int32, (blk, blk), 1)
     upper = jnp.where(r_i <= c_i, 1.0, 0.0).astype(F32)
@@ -433,7 +545,8 @@
         lax.broadcasted_iota(jnp.int32, (hp, cw), 1) // hd == lax.broadcasted_iota(jnp.int32, (hp, cw), 0), 1.0, 0.0
     ).astype(F32)
     skips = jnp.dot(
-        jnp.broadcast_to(skip[...], (8, heads)), expand[0:heads, :], precision=HIGH, preferred_element_type=F32
+        jnp.broadcast_to(par[0, 19:20, 0:heads], (8, heads)), expand[0:heads, :],
+        precision=HIGH, preferred_element_type=F32,
     )[0:1, :]
     eye_st = jnp.where(
         lax.broadcasted_iota(jnp.int32, (st, st), 0) == lax.broadcasted_iota(jnp.int32, (st, st), 1), 1.0, 0.0
@@ -455,22 +568,23 @@
         cum_cs.append(cum_c)
         st_rs.append(st_r)
 
+    oslice(2)
+
     @pl.when(me > 0)
     def _():
-        halo().wait_recv()
-        ext[0:raw0, :] = hrecv[...].astype(F32)
+        halo(hvs, hvr, 0).wait_recv()
+        extv[0:raw0, :] = hvr[...].astype(F32)
 
     @pl.when(me == 0)
     def _():
-        ext[0:raw0, :] = jnp.zeros((raw0, ext.shape[1]), F32)
-
-    width = taps_v.shape[0]
+        extv[0:raw0, :] = jnp.zeros((raw0, vc), F32)
+
     for b in range(blocks):
-        for taps, lo, hi in ((taps_v, 0, cw), (taps_k, cw, cw + st), (taps_r, cw + st, cw + 2 * st)):
+        for lo, hi in ((0, cw), (cw, vc)):
             total = jnp.zeros((blk, hi - lo), F32)
             for k in range(width):
                 o = b * blk + raw0 - (width - 1) + k
-                total = total + taps[k : k + 1, :] * ext[o : o + blk, cw + lo : cw + hi]
+                total = total + par[0, 24 + k : 25 + k, lo:hi] * extv[o : o + blk, lo:hi]
             conv[b * blk : (b + 1) * blk, lo:hi] = (total * jax.nn.sigmoid(total)).astype(BF)
 
     run = jnp.zeros((st, cw), F32)
@@ -514,31 +628,31 @@
 
     def pool(b):
         rows = slice(b * blk, (b + 1) * blk)
-        sums = jnp.dot(band, ext[b * blk : (b + 1) * blk + raw0, 0:cw].astype(BF), preferred_element_type=F32)
+        sums = jnp.dot(band, extp[b * blk : (b + 1) * blk + raw0, :].astype(BF), preferred_element_type=F32)
         pos = (me * n + b * blk + lax.broadcasted_iota(jnp.int32, (blk, cw), 0)).astype(F32)
         counts = jnp.minimum(pos + 1.0, window.astype(F32))
-        pooled = (sums / counts - ext[b * blk + raw0 : (b + 1) * blk + raw0, 0:cw]).astype(BF)
-        brow[rows, 0:cw] = (jnp.dot(pooled, mix[0], preferred_element_type=F32) * scale[...]).astype(BF)
-
-    work = [functools.partial(inner, b) for b in range(blocks)] + [functools.partial(pool, b) for b in range(blocks)]
+        pooled = (sums / counts - extp[b * blk + raw0 : (b + 1) * blk + raw0, :]).astype(BF)
+        pbuf[pslot, rows, :] = (
+            jnp.dot(pooled, mixb[0], preferred_element_type=F32) * par[0, 16:17, 0:cw]
+        ).astype(BF)
+
+    def xpeer(bit):
+        return {"c_": 1 - c} if bit == 1 else {"z_": flip(z, bit // 2)}
+
+    work = [functools.partial(inner, b) for b in range(blocks)]
     share = -(-len(work) // len(rounds))
-    o_left = [(op, 1), (oq, even[0])] + [(op, m) for m in early_first(S)] + [(oq, m) for m in even[1:]]
-    o_step = -(-len(o_left) // len(rounds))
-    o_rest = [(op, m) for m in masks if (op, m) not in o_left] + [(oq, m) for m in odd]
-
-    def take_o(count):
-        for stream, mask in o_left[:count]:
-            stream.got(mask)
-        del o_left[:count]
-
     for r, bit in enumerate(rounds):
         xs[r, 0:st, :] = run
         xs[r, st:, :] = jnp.broadcast_to(dec, (xs.shape[1] - st, cw))
-        send(xs.at[r], xr.at[r], x_ss.at[r], x_rs.at[r], sp=flip(me, bit))
+        copy(xs.at[r], xr.at[r], x_ss.at[r], x_rs.at[r], **xpeer(bit)).start()
         for f in work[r * share : (r + 1) * share]:
             f()
-        take_o(o_step)
-        remote(xs.at[r], xr.at[r], x_ss.at[r], x_rs.at[r], sp=flip(me, bit)).wait_recv()
+        if r == 0:
+            oslice(3)
+            pump(1, 3, start)
+        if r == 1:
+            oslice(4)
+        copy(xs.at[r], xr.at[r], x_ss.at[r], x_rs.at[r], **xpeer(bit)).wait_recv()
         other, odec = xr[r, 0:st, :], xr[r, st : st + 1, :]
         later = lax.rem(lax.div(me, bit), 2) == 1
         in_s = jnp.where(later, other * in_d + in_s, in_s)
@@ -551,83 +665,152 @@
         top, low = halves(pres[b] + offs[b] * in_s)
         rd = conv[rows, cw + st :]
         carried = jnp.dot(rd, top, preferred_element_type=F32) + jnp.dot(rd, low, preferred_element_type=F32)
-        y = scan[rows, :] + carried * expd[rows, :] + skips * conv[rows, 0:cw].astype(F32)
-        gt = acc[rows, cw : 2 * cw].astype(BF).astype(F32)
-        gated = y * (gt * jax.nn.sigmoid(gt))
-        ssend[:, rows] = bt(jnp.ones((8, cw), F32), gated * gated, precision=HIGH)
-        brow[rows, cw:] = (gated * sgain[...]).astype(BF)
-    for k in range(1, T):
-        send(ssend, srecv.at[k - 1], q_ss.at[k - 1], q_rs.at[k - 1], tp=flip(tp, k))
-    take_o(len(o_left))
-    for stream, mask in o_rest:
-        stream.got(mask)
-    for k in range(1, T):
-        remote(ssend, srecv.at[k - 1], q_ss.at[k - 1], q_rs.at[k - 1], tp=flip(tp, k)).wait_recv()
-    sq = ssend[...]
-    for k in range(1, T):
-        sq = sq + srecv[k - 1]
+        scan[rows, :] = scan[rows, :] + carried * expd[rows, :] + skips * conv[rows, 0:cw].astype(F32)
+
+    partners(1)
+    for r0 in range(0, n, mt):
+        d = jnp.dot(nbuf[0, r0 : r0 + mt, :], gbuf[0], preferred_element_type=F32)
+        for i in range(1, S):
+            d = d + jnp.dot(nbuf[i, r0 : r0 + mt, :], gbuf[i], preferred_element_type=F32)
+        low = d.astype(BF)
+        extp[raw0 + r0 : raw0 + r0 + mt, :] = low[:, 0:cw].astype(F32)
+        gateb[r0 : r0 + mt, :] = low[:, cw:]
+        if r0 + mt == n:
+            hps[...] = low[mt - raw0 :, 0:cw]
+
+    @pl.when(me < S - 1)
+    def _():
+        halo(hps, hpr, 1).start()
+
+    for b in range(blocks):
+        rows = slice(b * blk, (b + 1) * blk)
+        gt = gateb[rows, :].astype(F32)
+        gated = scan[rows, :] * (gt * jax.nn.sigmoid(gt))
+        sq_buf[pslot, :, rows] = bt(jnp.ones((8, cw), F32), gated * gated, precision=HIGH)
+        sbuf[pslot, rows, :] = (gated * par[0, 16:17, cw : 2 * cw]).astype(BF)
+
+    rows_of = (sbuf, pbuf)
+
+    def rcopy(k, r, way, src=None):
+        to = ({"c_": 1 - c}, {"x_": 1 - x}, {"y_": 1 - y})[way]
+        src = rows_of[k].at[r] if src is None else src
+        return copy(src, rows_of[k].at[r], p_ss.at[(k * T + r) * 3 + way], p_rs.at[k * T + r], **to)
+
+    def qcopy(i):
+        to = ({"c_": 1 - c}, {"x_": 1 - x}, {"x_": 1 - x, "c_": 1 - c}, {})[i]
+        return copy(sq_buf.at[pslot], sq_buf.at[tp], q_ss.at[i], q_rs.at[tp], **{"y_": c, **to})
+
+    def rows_out(k, do):
+        @pl.when(moved)
+        def _():
+            do(rcopy(k, tp, 2, rows_of[k].at[T]))
+
+        @pl.when(kept)
+        def _():
+            do(rcopy(k, tp, 1))
+            do(rcopy(k, tp, 0))
+
+    def rows_on(k, do, wait=True):
+        @pl.when(kept)
+        def _():
+            other = 2 * x + 1 - y
+            if wait:
+                rcopy(k, other, 0).wait_recv()
+            do(rcopy(k, other, 1))
+            do(rcopy(k, other, 0))
+            for r in (2 * (1 - x) + y, 2 * (1 - x) + 1 - y):
+                if wait:
+                    rcopy(k, r, 0).wait_recv()
+                do(rcopy(k, r, 0))
+
+    def squares(do):
+        for i in range(3):
+            do(qcopy(i))
+
+        @pl.when(moved)
+        def _():
+            do(qcopy(3))
+
+    squares(start)
+    rows_out(0, start)
+    oslice(5)
+
+    @pl.when(me > 0)
+    def _():
+        halo(hps, hpr, 1).wait_recv()
+        extp[0:raw0, :] = hpr[...].astype(F32)
+
+    @pl.when(me == 0)
+    def _():
+        extp[0:raw0, :] = jnp.zeros((raw0, cw), F32)
+
+    for b in range(blocks):
+        pool(b)
+    rows_out(1, start)
+    rows_on(0, start)
+    oslice(6)
+    rows_on(1, start)
+
+    @pl.when(moved)
+    def _():
+        for k in range(2):
+            for r in range(T):
+                rcopy(k, r, 0).wait_recv()
+
+    for r in range(T):
+        @pl.when((tp != r) | moved)
+        def _():
+            copy(sq_buf.at[r], sq_buf.at[r], q_ss.at[0], q_rs.at[r], c_=1 - c).wait_recv()
+
+    for q in range(T):
+        ref = obuf.at[(1 - y) * T + q]
+        copy(ref, ref, o_ss.at[0], o_rs.at[(1 - y) * T + q], y_=1 - y).wait_recv()
+
+    sq = sum(sq_buf[r] for r in range(T))
     rs_row = lax.rsqrt(sq / (cw * T) + EPSILON)
     rs_cols = [bt(eye, rs_row[:, b * blk : (b + 1) * blk], precision=HIGH)[:, 0:1] for b in range(blocks)]
-    wide = S // T
-    oc = obuf.shape[2]
-    parts = 4
-    pr = n // parts
-
-    def product(t, part, store):
-        rows = slice(part * pr, (part + 1) * pr)
-        rs = jnp.concatenate(rs_cols[part * blocks // parts : (part + 1) * blocks // parts], axis=0)
-        for j in range(wide):
-            i = t * wide + j
-            p = jnp.dot(brow[rows, 0:cw], obuf[i, 0:cw, :], preferred_element_type=F32)
-            p = p + rs * jnp.dot(brow[rows, cw:], obuf[i, cw:, :], preferred_element_type=F32)
-            store(rows, slice(j * oc, (j + 1) * oc), p)
-
-    def into(ref, *lead):
-        def store(rows, cols, p):
-            ref[lead + (rows, cols)] = p.astype(ref.dtype)
-        return store
-
-    near = flip(tp, 1)
-
-    def near_copy(k, part):
-        rows = pl.ds(part * pr, pr)
-        i = k * parts + part
-        return remote(psend.at[k, rows], precv.at[k, rows], p_ss.at[i], p_rs.at[i], tp=near)
-
-    def far_copy(part):
-        rows = pl.ds(part * pr, pr)
-        return remote(qsend.at[rows], qrecv.at[rows], r_ss.at[part], r_rs.at[part], tp=flip(tp, 2))
-
-    for part in range(parts):
-        product(flip(tp, 3), part, into(psend, 0))
-        near_copy(0, part).start()
-    for part in range(parts):
-        rows = slice(part * pr, (part + 1) * pr)
-        product(flip(tp, 2), part, into(pown))
-        near_copy(0, part).wait_recv()
-        qsend[rows, :] = (pown[rows, :] + precv[0, rows, :]).astype(BF)
-        far_copy(part).start()
-    for part in range(parts):
-        product(near, part, into(psend, 1))
-        near_copy(1, part).start()
-    for part in range(parts):
-        product(tp, part, into(pown))
-    for part in range(parts):
-        rows = slice(part * pr, (part + 1) * pr)
-        near_copy(1, part).wait_recv()
-        far_copy(part).wait_recv()
-        out[rows, :] = (pown[rows, :] + precv[1, rows, :] + qrecv[rows, :].astype(F32)).astype(out.dtype)
-
-    for c in started:
-        c.wait_send()
-    for part in range(parts):
-        near_copy(0, part).wait_send()
-        near_copy(1, part).wait_send()
-        far_copy(part).wait_send()
+    for r0 in range(0, n, mt):
+        rows = slice(r0, r0 + mt)
+        rs = jnp.concatenate(rs_cols[r0 // blk : (r0 + mt) // blk], axis=0)
+        for j in range(2):
+            p = jnp.dot(pbuf[0, rows, :], obuf[j * T, 0:cw, :], preferred_element_type=F32)
+            s = jnp.dot(sbuf[0, rows, :], obuf[j * T, cw:, :], preferred_element_type=F32)
+            for q in range(1, T):
+                p = p + jnp.dot(pbuf[q, rows, :], obuf[j * T + q, 0:cw, :], preferred_element_type=F32)
+                s = s + jnp.dot(sbuf[q, rows, :], obuf[j * T + q, cw:, :], preferred_element_type=F32)
+            out[rows, j * oc : (j + 1) * oc] = (p + rs * s).astype(out.dtype)
+
+    for k in range(2):
+        source(k, done)
+        for d in range(1, Z):
+            pump(k, d, done, wait=False)
+        rows_out(k, done)
+        rows_on(k, done, wait=False)
+    for q in range(T):
+        omoves(q, done)
+    squares(done)
+    acopy(1).wait_send()
+    acopy(2).wait_send()
+
+    @pl.when(moved)
+    def _():
+        acopy(0).wait_send()
+        for i in range(4):
+            swap(i).wait_send()
+        for f in range(2):
+            aforward(f).wait_send()
+
+    @pl.when(jnp.logical_not(hub))
+    def _():
+        ohub().wait_send()
+
+    for r, bit in enumerate(rounds):
+        copy(xs.at[r], xr.at[r], x_ss.at[r], x_rs.at[r], **xpeer(bit)).wait_send()
 
     @pl.when(me < S - 1)
     def _():
-        halo().wait_send()
+        halo(hvs, hvr, 0).wait_send()
+        halo(hps, hpr, 1).wait_send()
 
 
 def fits(S, T, shapes):
@@ -636,11 +819,12 @@
     st = shapes[5][1]
     oc = shapes[18][1]
     heads = shapes[7][1]
+    taps = shapes[10][0]
     return (
-        T == 4 == POOL_GROUPS and S >= T and S & (S - 1) == 0 and S <= 16 and st == SSM_STATE
-        and cw == heads * SSM_STATE and n % (4 * SCAN_BLOCK) == 0
-        and -(-kd // 96) * 2 * cw % kd == 0 and oc % 128 == 0 and kd % 128 == 0 and da % kd == 0
-        and n % (2 * SCAN_BLOCK) == 0 and cw % 128 == 0 and oc * S == da * T
+        T == 4 == POOL_GROUPS and S == 2 * T and st == SSM_STATE and taps <= 8 and heads <= 8
+        and cw == heads * SSM_STATE and n % 256 == 0 and n % SCAN_BLOCK == 0 and n >= 2 * cw
+        and oc % 128 == 0 and kd % 128 == 0 and da % kd == 0 and da * T == kd * S and kd <= cw + 2 * st
+        and cw % 128 == 0 and oc * 2 == da
     )
 
 
@@ -652,7 +836,6 @@
     n, da = activations.shape
     kd, cw = pool_weight.shape
     st = key_weight.shape[1]
-    heads = step_weight.shape[1]
     oc = out_pool_weight.shape[1]
     hp = 16
     args = (
@@ -661,20 +844,19 @@
         decay_extra.T, skip_scale[None, :], state_gain[None, :],
         out_pool_weight, out_state_weight,
     )
-    ncol = 3 * cw + 2 * st
-    ccol = ncol - cw
+    vc = cw + 2 * st
     V = pltpu.VMEM
     D = pltpu.SemaphoreType.DMA
     R = S.bit_length() - 1
     scratch = [
-        V((S, kd, ncol), BF), V((S, hp, kd), BF), V((S, 2 * cw, oc), BF), V((T, n + 16, da), BF),
-        V((S, n, kd), BF), V((n, ncol), F32), V((hp, n), F32), V((n + 16, ccol), F32),
-        V((n, cw + 2 * st), BF), V((16, ccol), BF), V((16, ccol), BF), V((n, cw), F32),
-        V((R, st + 8, cw), F32), V((R, st + 8, cw), F32), V((8, n), F32), V((T - 1, 8, n), F32),
-        V((n, 2 * cw), BF), V((2, n, da), F32), V((2, n, da), F32), V((n, da), F32),
-        V((n, da), BF), V((n, da), BF), V((n, cw), F32),
-        D((2 * S,)), D((2 * S,)), D((S,)), D((S,)), D((2 * S,)), D((2 * S,)), D((T,)), D((T,)), D, D,
-        D((R,)), D((R,)), D((T,)), D((T,)), D((8,)), D((8,)), D((4,)), D((4,)),
+        V((S + 1, kd + hp, vc), BF), V((S + 1, kd, 2 * cw), BF), V((2 * T + 1, 2 * cw, oc), BF),
+        V((T + 1, n + 16, da), BF), V((2, cw, cw), BF), V((2, 32, n), F32),
+        V((S, n, kd), BF), V((n + 16, vc), F32), V((n + 16, cw), F32), V((n, cw), BF), V((n, vc), BF),
+        V((16, vc), BF), V((16, vc), BF), V((16, cw), BF), V((16, cw), BF), V((n, cw), F32),
+        V((R, st + 8, cw), F32), V((R, st + 8, cw), F32),
+        V((T + 1, 8, n), F32), V((T + 1, n, cw), BF), V((T + 1, n, cw), BF), V((n, cw), F32),
+        D((6 * S,)), D((2 * S,)), D((1 + 3 * T,)), D((2 * T,)), D((5,)), D((T,)), D((4,)), D((2,)),
+        D((2,)), D((2,)), D((R,)), D((R,)), D((4,)), D((T,)), D((6 * T,)), D((2 * T,)),
     ]
     return pl.pallas_call(
         functools.partial(mixer_kernel, S, T),

time: 102 us -> 94.8 us (0.929)
  Pallas kernels: 98.4 us -> 91.5 us
    pallas_call x1, Pallas kernels: 98.4 us -> 91.5 us  [fused(): pl.pallas_call(functools.partial(mixer_kernel, S, T), out_shape=jax.Shape...]
where the time goes in v1:
time: 94.8 us; the launch traced here: 94.6 us
  Pallas kernels  91.5 us (97%)
  local copies, waits for them, and re-layouts  3.13 us (3%)
    pallas_call x1, Pallas kernels, fused(): pl.pallas_call(functools.partial(mixer_kernel, S, T), out_shape=jax.Shape...  91.5 us
    unnamed x3, local copies, waits for them, and re-layouts  2.55 us

profile of v1, /device:TPU:1, one launch (start us, length us, event | category | flops | bytes accessed | tf_op | source)
XLA Modules:
  0.0 94.6 jit_solution(5303440916403906657)
XLA Ops:
  0.0 0.0 copy-start
  0.0 0.7 copy-done
  0.7 0.6 broadcast_in_dim.18.gain
  1.3 91.5 %shard_map.190 = bf16[512,512]{1,0:T(8,128)(2,1)} custom-call(bf16[512,512]{1,0:T(8,128)(2,1)} %act.1, bf16[1,512]{1,0:T(2,128)(2,1)} %broadcast_in_dim.18.gain, bf16[256,256]{1,0:T(8,128)(2,1)} %pool_w.1, bf16[256,256]{1,0:T(8,128)(2,1)} %gate_w.1, bf16[256,256]{1,0:T(8,128)(2,1)} %value_w.1, bf16[64,256]{1,0:T(8,128)(2,1)} %bitcast.9, ...), custom_call_target="tpu_custom_call" | custom-call | tf_op jit(solution)/shard_map/pallas_call | solution.py:861
  92.7 1.9 %copy.22 = bf16[512,512]{1,0:T(8,128)(2,1)} copy(bf16[512,512]{1,0:T(8,128)(2,1)} %shard_map.190) | data formatting | bytes 1048576
Async XLA Ops:
  0.0 0.7 copy-start

commit v2 on v1

--- a/solution.py
+++ b/solution.py
@@ -234,7 +234,7 @@
     act, gain, pool_w, gate_w, value_w, key_w, read_w, step_t, mix, scale, taps_v, taps_k, taps_r,
     bias, dlog, extra_t, skip, sgain, opool, ostate,
     out,
-    vbuf, gbuf, obuf, abuf, mixb, par, nbuf, extv, extp, gateb, conv, hvs, hvr, hps, hpr, scan, xs, xr,
+    vbuf, gbuf, obuf, abuf, mixb, par, nbuf, extv, extp, gateb, conv, hbuf, scan, xs, xr,
     sq_buf, pbuf, sbuf, expd,
     b_ss, b_rs, o_ss, o_rs, a_ss, a_rs, t_ss, t_rs, h_ss, h_rs, x_ss, x_rs, q_ss, q_rs, p_ss, p_rs,
 ):
@@ -258,8 +258,10 @@
     slot = me + off * (S - me)
     aslot = tq + off * (T - tq)
     pslot = tp + off * (T - tp)
-    hub = tq == z
-    oslot = jnp.where(hub, y * T + tq, 2 * T)
+    hubs = (tq == z, 2 * (1 - x) + c == z)
+    hub = hubs[0] | hubs[1]
+    turn = lax.rem(y + c, 2)
+    oslot = jnp.where(hubs[0], y * T + tq, jnp.where(hubs[1], 2 * T + 1 + turn, 2 * T))
 
     def dev(z_=z, y_=y, x_=x, c_=c):
         return {"sp": 2 * z_ + y_, "tp": 2 * x_ + c_}
@@ -268,6 +270,19 @@
         return pltpu.make_async_remote_copy(
             src_ref=src, dst_ref=dst, send_sem=ss, recv_sem=rs, device_id=dev(**to), device_id_type=MESH
         )
+
+    barrier = pltpu.get_barrier_semaphore()
+
+    def greet(**to):
+        pl.semaphore_signal(barrier, inc=1, device_id=dev(**to), device_id_type=MESH)
+
+    for dz in range(Z):
+        for k in range(8):
+            if dz or k:
+                greet(
+                    z_=lax.rem(z + dz, Z), y_=1 - y if k & 4 else y, x_=1 - x if k & 2 else x,
+                    c_=1 - c if k & 1 else c,
+                )
 
     eye_kd = jnp.where(
         lax.broadcasted_iota(jnp.int32, (kd, kd), 0) == lax.broadcasted_iota(jnp.int32, (kd, kd), 1), 1.0, 0.0
@@ -282,18 +297,6 @@
     abuf[aslot, 0:n, :] = act[...]
     abuf[aslot, n : n + 16, :] = jnp.broadcast_to(gain[...].astype(F32), (16, da)).astype(BF)
 
-    barrier = pltpu.get_barrier_semaphore()
-
-    def greet(**to):
-        pl.semaphore_signal(barrier, inc=1, device_id=dev(**to), device_id_type=MESH)
-
-    for k in range(1, 8):
-        greet(
-            y_=1 - y if k & 4 else y, x_=1 - x if k & 2 else x, c_=1 - c if k & 1 else c,
-        )
-    for k in range(1, Z):
-        greet(z_=lax.rem(z + k, Z))
-        greet(z_=lax.rem(z + k, Z), c_=1 - c)
     gbuf[slot, :, 0:cw] = pool_w[...]
     gbuf[slot, :, cw:] = gate_w[...]
     obuf[oslot, 0:cw, :] = opool[...]
@@ -310,26 +313,38 @@
     par[off, 24 : 24 + width, 0:cw] = taps_v[...]
     par[off, 24 : 24 + width, cw : cw + st] = taps_k[...]
     par[off, 24 : 24 + width, cw + st : vc] = taps_r[...]
-    pl.semaphore_wait(barrier, 7 + 2 * (Z - 1))
-
+    pl.semaphore_wait(barrier, S * T - 1)
+
+    raw0 = hbuf.shape[1]
+    own_halo = (y == 0) & (c == 1)
+
+    @pl.when(own_halo)
+    def _():
+        hbuf[tq] = act[n - raw0 :, :]
+
+    @pl.when(me == 0)
+    def _():
+        hbuf[...] = jnp.zeros(hbuf.shape, BF)
+
+    middle = (z == 1) | (z == Z - 2)
     streams = (vbuf, gbuf)
 
     def bcopy(k, i, way):
-        to = ({"c_": 1 - c}, {"z_": z + 1}, {"z_": z - 1})[way]
+        to = ({"c_": 1 - c}, {"z_": z + 1}, {"z_": z - 1}, {"z_": z + 2}, {"z_": z - 2})[way]
         ref = streams[k].at[i]
-        return copy(ref, ref, b_ss.at[(k * S + i) * 3 + way], b_rs.at[k * S + i], **to)
+        return copy(ref, ref, b_ss.at[(k * S + i) * 5 + way], b_rs.at[k * S + i], **to)
 
     def arrived(k, i):
         bcopy(k, i, 0).wait_recv()
 
     def source(k, do):
-        @pl.when(z < Z - 1)
-        def _():
-            do(bcopy(k, me, 1))
-
-        @pl.when(z > 0)
-        def _():
-            do(bcopy(k, me, 2))
+        ways = [(1, z < Z - 1), (2, z > 0)]
+        if k:
+            ways = [(3, moved & (z == 0)), (4, moved & (z == Z - 1))] + ways
+        for way, when in ways:
+            @pl.when(when)
+            def _():
+                do(bcopy(k, me, way))
 
         do(bcopy(k, me, 0))
 
@@ -339,26 +354,30 @@
     def done(d):
         d.wait_send()
 
-    def pump(k, d, do, wait=True):
-        @pl.when(z >= d)
+    def pump(k, d, do, wait=True, when=True):
+        right, left = z < Z - 1, z > 0
+        if k and d == 1:
+            right, left = right & (kept | (z > 1)), left & (kept | (z < Z - 2))
+
+        @pl.when((z >= d) & when)
         def _():
             i = 2 * (z - d) + c
             if wait:
                 arrived(k, i)
 
-            @pl.when(z < Z - 1)
+            @pl.when(right)
             def _():
                 do(bcopy(k, i, 1))
 
             do(bcopy(k, i, 0))
 
-        @pl.when(z + d < Z)
+        @pl.when((z + d < Z) & when)
         def _():
             i = 2 * (z + d) + c
             if wait:
                 arrived(k, i)
 
-            @pl.when(z > 0)
+            @pl.when(left)
             def _():
                 do(bcopy(k, i, 2))
 
@@ -381,67 +400,171 @@
         to = ({"c_": y}, {"x_": 1 - x, "c_": y}, {"y_": 1 - y, "c_": y})[way]
         return copy(abuf.at[aslot], abuf.at[tq], a_ss.at[way], a_rs.at[tq], **to)
 
-    def aforward(f):
-        t = 2 * x + f
-        return copy(abuf.at[t], abuf.at[t], a_ss.at[3 + f], a_rs.at[t], x_=1 - x)
+    def aforward(i):
+        t, to = ((2 * x + 1 - c, {"x_": 1 - x}), (2 * (1 - x) + c, {"y_": 1 - y}))[i]
+        return copy(abuf.at[t], abuf.at[t], a_ss.at[3 + i], a_rs.at[t], **to)
 
     def agot(t):
         copy(abuf.at[t], abuf.at[t], a_ss.at[0], a_rs.at[t], x_=1 - x).wait_recv()
 
+    def hcopy(k):
+        return copy(
+            abuf.at[aslot, pl.ds(n - raw0, raw0)], hbuf.at[tq], h_ss.at[k], h_rs.at[tq],
+            z_=z + y, y_=k // 2, x_=k % 2, c_=1 - y,
+        )
+
+    def hsends(do):
+        @pl.when(sp < S - 1)
+        def _():
+            for k in range(4):
+                @pl.when(jnp.logical_not(own_halo & (y == k // 2) & (x == k % 2)))
+                def _():
+                    do(hcopy(k))
+
+    def hgot():
+        @pl.when(me > 0)
+        def _():
+            for t in range(T):
+                @pl.when(jnp.logical_not(own_halo & (tq == t)))
+                def _():
+                    copy(hbuf.at[t], hbuf.at[t], h_ss.at[0], h_rs.at[t], x_=1 - x).wait_recv()
+
+    def oquarter(j):
+        return 2 * x + (y if j == 0 else 1 - y)
+
+    def oslots(line, j):
+        return 2 * T + 1 + j if line else y * T + oquarter(j)
+
     def ohub():
-        return copy(
-            obuf.at[2 * T], obuf.at[y * T + tq], o_ss.at[0], o_rs.at[y * T + tq], x_=lax.div(z, 2), c_=lax.rem(z, 2)
-        )
-
-    def ocopy(q, way):
-        to = ({"y_": 1 - y}, {"z_": z + 1}, {"z_": z - 1})[way]
-        ref = obuf.at[y * T + q]
-        return copy(ref, ref, o_ss.at[1 + q * 3 + way], o_rs.at[y * T + q], **to)
-
-    def omoves(q, do):
-        @pl.when((z >= tq) & (z < Z - 1))
-        def _():
-            do(ocopy(q, 1))
-
-        @pl.when((z <= tq) & (z > 0))
-        def _():
-            do(ocopy(q, 2))
-
-        do(ocopy(q, 0))
-
-    def oslice(tau):
-        for q in range(T):
-            d = tau - q
-            if d == 0:
-                @pl.when(hub)
+        home = lax.div(z, 2) == x
+        dst = jnp.where(home, y * T + tq, 2 * T + 1 + turn)
+        return copy(obuf.at[2 * T], obuf.at[dst], o_ss.at[0], o_rs.at[dst], c_=1 - c)
+
+    def ocopy(line, j, way):
+        to = (
+            {"z_": z + 1}, {"z_": z - 1}, {"z_": z + 2}, {"z_": z - 2},
+            {"x_": 1 - x} if line else {"y_": 1 - y},
+        )[way]
+        i = oslots(line, j)
+        dst = i if way < 4 else y * T + oquarter(j)
+        return copy(obuf.at[i], obuf.at[dst], o_ss.at[1 + (2 * line + j) * 6 + way], o_rs.at[dst], **to)
+
+    def owait(line, j):
+        i = oslots(line, j)
+        copy(obuf.at[i], obuf.at[i], o_ss.at[0], o_rs.at[i], x_=1 - x).wait_recv()
+
+    def across(line, j, do):
+        if not line:
+            do(ocopy(line, j, 4))
+
+    def over(line, j, do):
+        if line:
+            do(ocopy(line, j, 4))
+
+    def osend(line, j, do):
+        for way, when in ((2, z == 0), (3, z == Z - 1), (0, middle), (1, middle)):
+            @pl.when(when)
+            def _():
+                do(ocopy(line, j, way))
+
+    def center(line):
+        return 2 * (1 - x) + c if line else tq
+
+    def relays(line):
+        h = center(line)
+        return ((z == Z - 2) & (h < 2)) | ((z == 1) & (h > 1))
+
+    def orelay(line, j, do):
+        h = center(line)
+        for way, when in ((0, h < 2), (1, h > 1), (1, h == 0), (0, h == T - 1)):
+            @pl.when(when)
+            def _():
+                do(ocopy(line, j, way))
+
+    def ofrom(j, when=True):
+        for line in range(2):
+            @pl.when(hubs[line] & when)
+            def _():
+                osend(line, j, start)
+
+    def ocross():
+        for line in range(2):
+            @pl.when(hubs[line])
+            def _():
+                for j in range(2):
+                    @pl.when(turn != j)
+                    def _():
+                        owait(line, j)
+
+                    over(line, j, start)
+                    across(line, j, start)
+
+    def opass(j):
+        for line in range(2):
+            @pl.when(relays(line))
+            def _():
+                owait(line, j)
+                orelay(line, j, start)
+                over(line, j, start)
+
+                @pl.when(kept)
                 def _():
-                    @pl.when(tq != q)
-                    def _():
-                        ocopy(q, 0).wait_recv()
-
-                    omoves(q, start)
-            elif 0 < d < Z:
-                @pl.when((z == tq + d) | (z == tq - d))
+                    across(line, j, start)
+
+    def olate():
+        for line in range(2):
+            @pl.when(relays(line) & moved)
+            def _():
+                for j in range(2):
+                    across(line, j, start)
+
+    def oend(line, j):
+        @pl.when(jnp.logical_not(hubs[line] | relays(line)))
+        def _():
+            owait(line, j)
+            over(line, j, start)
+            across(line, j, start)
+
+    def ofar(j, do, wait=True):
+        i = y * T + 2 * (1 - x) + (y if j == 0 else 1 - y)
+        d = copy(obuf.at[i], obuf.at[i], o_ss.at[25 + j], o_rs.at[i], y_=1 - y)
+        if wait:
+            d.wait_recv()
+        do(d)
+
+    def oall(do):
+        for j in range(2):
+            ofar(j, do, False)
+
+        for line in range(2):
+            for j in range(2):
+                @pl.when(hubs[line])
                 def _():
-                    ocopy(q, 0).wait_recv()
-                    omoves(q, start)
+                    osend(line, j, do)
+
+                @pl.when(relays(line))
+                def _():
+                    orelay(line, j, do)
+
+                over(line, j, do)
+                across(line, j, do)
 
     @pl.when(moved)
     def _():
         swap(0).start()
 
     acopy(1).start()
-    acopy(2).start()
-
-    @pl.when(moved)
-    def _():
+    hsends(start)
+
+    @pl.when(moved)
+    def _():
+        acopy(2).start()
         acopy(0).start()
-        for i in range(1, 4):
-            swap(i).start()
-
-    @pl.when(jnp.logical_not(hub))
-    def _():
-        ohub().start()
+        swap(2).start()
+
+        @pl.when(jnp.logical_not(hub))
+        def _():
+            ohub().start()
 
     @pl.when(moved)
     def _():
@@ -453,43 +576,57 @@
     def _():
         source(1, start)
 
-    @pl.when(moved)
-    def _():
-        agot(2 * x + c)
-        aforward(c).start()
-
     pump(0, 1, start)
 
+    @pl.when(kept)
+    def _():
+        acopy(2).start()
+        agot(2 * (1 - x) + c)
+        aforward(1).start()
+
+        @pl.when(jnp.logical_not(hub))
+        def _():
+            ohub().start()
+
     @pl.when(moved)
     def _():
         agot(2 * x + 1 - c)
-        aforward(1 - c).start()
+        aforward(0).start()
 
     pump(0, 2, start)
 
-    @pl.when(moved)
-    def _():
+    pump(0, 3, start)
+
+    @pl.when(moved)
+    def _():
+        swap(1).start()
+        swap(3).start()
         arrived(1, me)
         source(1, start)
 
-    oslice(0)
-    pump(1, 1, start)
-    pump(0, 3, start)
+    @pl.when(kept)
+    def _():
+        pump(1, 1, start)
+
     partners(0)
 
     @pl.when(kept)
     def _():
         agot(2 * x + 1 - c)
 
-    agot(2 * (1 - x))
-    agot(2 * (1 - x) + 1)
-
+    @pl.when(moved)
+    def _():
+        agot(2 * x + c)
+        agot(2 * (1 - x) + c)
+
+    agot(2 * (1 - x) + 1 - c)
+    hgot()
+
+    ocross()
     per = da // kd
     rt = 64
 
-    def norm_rows(i, _):
-        r = pl.ds(pl.multiple_of(i * rt, rt), rt)
-        parts = [abuf[t, r, :].astype(F32) for t in range(T)]
+    def norm_rows(parts, r):
         tot = sum(jnp.sum(p * p, axis=-1, keepdims=True) for p in parts)
         rs = lax.rsqrt(tot / (da * T) + EPSILON)
         for t in range(T):
@@ -497,33 +634,48 @@
             v = (parts[t] * rs * g).astype(BF)
             for j in range(per):
                 nbuf[t * per + j, r, :] = v[:, j * kd : (j + 1) * kd]
+
+    def norm_tile(i, _):
+        r = pl.ds(pl.multiple_of(i * rt, rt), rt)
+        norm_rows([abuf[t, r, :].astype(F32) for t in range(T)], r)
         return 0
 
-    lax.fori_loop(0, n // rt, norm_rows, 0)
+    lax.fori_loop(0, n // rt, norm_tile, 0)
+    norm_rows([hbuf[t].astype(F32) for t in range(T)], pl.ds(n, raw0))
+    @pl.when(moved)
+    def _():
+        pump(1, 1, start)
+
+
     mt = 256
-    raw0 = 16
-
-    for r0 in range(0, n, mt):
-        d = jnp.dot(nbuf[0, r0 : r0 + mt, :], vbuf[0, 0:kd, :], preferred_element_type=F32)
+
+    def tiles():
+        for r0 in range(0, n, mt):
+            yield r0, slice(r0, r0 + mt + raw0 if r0 + mt == n else r0 + mt)
+
+    def keep(ref, r0, low):
+        ref[raw0 + r0 : raw0 + r0 + mt, :] = low[0:mt, :].astype(F32)
+        if low.shape[0] > mt:
+            ref[0:raw0, :] = low[mt:, :].astype(F32)
+
+    for r0, rows in tiles():
+        d = jnp.dot(nbuf[0, rows, :], vbuf[0, 0:kd, :], preferred_element_type=F32)
         for i in range(1, S):
-            d = d + jnp.dot(nbuf[i, r0 : r0 + mt, :], vbuf[i, 0:kd, :], preferred_element_type=F32)
-        low = d.astype(BF)
-        extv[raw0 + r0 : raw0 + r0 + mt, :] = low.astype(F32)
-        if r0 + mt == n:
-            hvs[...] = low[mt - raw0 :, :]
-
-    def halo(src, dst, i):
-        return copy(src, dst, h_ss.at[i], h_rs.at[i], z_=z + c, c_=1 - c)
-
-    @pl.when(me < S - 1)
-    def _():
-        halo(hvs, hvr, 0).start()
-
-    sacc = bt(vbuf[0, kd:, 0:kd], nbuf[0])
+            d = d + jnp.dot(nbuf[i, rows, :], vbuf[i, 0:kd, :], preferred_element_type=F32)
+        keep(extv, r0, d.astype(BF))
+
+    sacc = bt(vbuf[0, kd:, 0:kd], nbuf[0, 0:n, :])
     for i in range(1, S):
-        sacc = sacc + bt(vbuf[i, kd:, 0:kd], nbuf[i])
-    oslice(1)
-    pump(1, 2, start)
+        sacc = sacc + bt(vbuf[i, kd:, 0:kd], nbuf[i, 0:n, :])
+    @pl.when(kept)
+    def _():
+        pump(1, 2, start)
+
+    @pl.when(moved)
+    def _():
+        pump(1, 2, start, when=middle)
+
+    ofrom(0)
 
     @pl.when(moved)
     def _():
@@ -568,16 +720,6 @@
         cum_cs.append(cum_c)
         st_rs.append(st_r)
 
-    oslice(2)
-
-    @pl.when(me > 0)
-    def _():
-        halo(hvs, hvr, 0).wait_recv()
-        extv[0:raw0, :] = hvr[...].astype(F32)
-
-    @pl.when(me == 0)
-    def _():
-        extv[0:raw0, :] = jnp.zeros((raw0, vc), F32)
 
     for b in range(blocks):
         for lo, hi in ((0, cw), (cw, vc)):
@@ -602,10 +744,6 @@
         run = run * bd + new
         dec = dec * bd
 
-    in_s = jnp.zeros((st, cw), F32)
-    in_d = jnp.ones((1, cw), F32)
-    rounds = [1 << k for k in range(S.bit_length() - 1)]
-
     def inner(b):
         rows = slice(b * blk, (b + 1) * blk)
         g = bt(conv[rows, cw + st :], conv[rows, cw : cw + st])
@@ -636,121 +774,150 @@
             jnp.dot(pooled, mixb[0], preferred_element_type=F32) * par[0, 16:17, 0:cw]
         ).astype(BF)
 
-    def xpeer(bit):
-        return {"c_": 1 - c} if bit == 1 else {"z_": flip(z, bit // 2)}
-
-    work = [functools.partial(inner, b) for b in range(blocks)]
-    share = -(-len(work) // len(rounds))
-    for r, bit in enumerate(rounds):
-        xs[r, 0:st, :] = run
-        xs[r, st:, :] = jnp.broadcast_to(dec, (xs.shape[1] - st, cw))
-        copy(xs.at[r], xr.at[r], x_ss.at[r], x_rs.at[r], **xpeer(bit)).start()
-        for f in work[r * share : (r + 1) * share]:
-            f()
-        if r == 0:
-            oslice(3)
-            pump(1, 3, start)
-        if r == 1:
-            oslice(4)
-        copy(xs.at[r], xr.at[r], x_ss.at[r], x_rs.at[r], **xpeer(bit)).wait_recv()
-        other, odec = xr[r, 0:st, :], xr[r, st : st + 1, :]
-        later = lax.rem(lax.div(me, bit), 2) == 1
-        in_s = jnp.where(later, other * in_d + in_s, in_s)
-        in_d = jnp.where(later, odec * in_d, in_d)
-        run = jnp.where(later, other * dec + run, run * odec + other)
-        dec = dec * odec
+    rows_of = (sbuf, pbuf)
+
+    def rcopy(k, r, way, src=None):
+        to = ({"c_": 1 - c}, {"x_": 1 - x}, {"y_": 1 - y})[way]
+        src = rows_of[k].at[r] if src is None else src
+        return copy(src, rows_of[k].at[r], p_ss.at[(k * T + r) * 3 + way], p_rs.at[k * T + r], **to)
+
+    def qcopy(i):
+        to = ({"c_": 1 - c}, {"x_": 1 - x}, {"x_": 1 - x, "c_": 1 - c}, {})[i]
+        return copy(sq_buf.at[pslot], sq_buf.at[tp], q_ss.at[i], q_rs.at[tp], **{"y_": c, **to})
+
+    def rows_out(k, do):
+        @pl.when(moved)
+        def _():
+            do(rcopy(k, tp, 2, rows_of[k].at[T]))
+
+        @pl.when(kept)
+        def _():
+            do(rcopy(k, tp, 1))
+            do(rcopy(k, tp, 0))
+
+    def rows_on(k, do, wait=True):
+        @pl.when(kept)
+        def _():
+            other = 2 * x + 1 - y
+            if wait:
+                rcopy(k, other, 0).wait_recv()
+            do(rcopy(k, other, 1))
+            do(rcopy(k, other, 0))
+
+    def rows_over(k, do, wait=True):
+        @pl.when(kept)
+        def _():
+            for r in (2 * (1 - x) + y, 2 * (1 - x) + 1 - y):
+                if wait:
+                    rcopy(k, r, 0).wait_recv()
+                do(rcopy(k, r, 0))
+
+    def squares(do):
+        for i in range(3):
+            do(qcopy(i))
+
+        @pl.when(moved)
+        def _():
+            do(qcopy(3))
+
+    def gates():
+        for r0, rows in tiles():
+            d = jnp.dot(nbuf[0, rows, :], gbuf[0], preferred_element_type=F32)
+            for i in range(1, S):
+                d = d + jnp.dot(nbuf[i, rows, :], gbuf[i], preferred_element_type=F32)
+            low = d.astype(BF)
+            keep(extp, r0, low[:, 0:cw])
+            gateb[r0 : r0 + mt, :] = low[0:mt, cw:]
+
+    def pools():
+        for b in range(blocks):
+            pool(b)
+        rows_out(1, start)
+
+    def xpair():
+        return copy(xs.at[0], xr.at[Z - 1], x_ss.at[0], x_rs.at[Z - 1], c_=1 - c)
+
+    def xline(k):
+        return copy(xs.at[1], xr.at[z], x_ss.at[k], x_rs.at[z], z_=z + k)
+
+    def xlines(do):
+        for k in reversed(range(1, Z)):
+            @pl.when(z + k < Z)
+            def _():
+                do(xline(k))
+
+    def put(i):
+        xs[i, 0:st, :] = run
+        xs[i, st:, :] = jnp.broadcast_to(dec, (xs.shape[1] - st, cw))
+
+    put(0)
+    xpair().start()
+
+    @pl.when(kept)
+    def _():
+        pump(1, 3, start)
+
+    @pl.when(moved)
+    def _():
+        pump(1, 2, start, when=jnp.logical_not(middle))
+
+    for b in range(blocks // 2):
+        inner(b)
+    xpair().wait_recv()
+    other, odec = xr[Z - 1, 0:st, :], xr[Z - 1, st : st + 1, :]
+    later = c == 1
+    own_s, own_d = jnp.where(later, other, 0.0), jnp.where(later, odec, 1.0)
+    run = jnp.where(later, other * dec + run, run * odec + other)
+    dec = dec * odec
+    put(1)
+    xlines(start)
+    ofrom(1)
+
+    for b in range(blocks // 2, blocks):
+        inner(b)
+    opass(0)
+
+    @pl.when(moved)
+    def _():
+        pump(1, 3, start)
+
+    partners(1)
+    gates()
+    pools()
+    opass(1)
+    in_s = jnp.zeros((st, cw), F32)
+    for p in range(Z - 1):
+        @pl.when(z > p)
+        def _():
+            copy(xs.at[1], xr.at[p], x_ss.at[1], x_rs.at[p], c_=1 - c).wait_recv()
+
+        in_s = jnp.where(z > p, in_s * xr[p, st : st + 1, :] + xr[p, 0:st, :], in_s)
+    in_s = in_s * own_d + own_s
 
     for b in range(blocks):
         rows = slice(b * blk, (b + 1) * blk)
         top, low = halves(pres[b] + offs[b] * in_s)
         rd = conv[rows, cw + st :]
         carried = jnp.dot(rd, top, preferred_element_type=F32) + jnp.dot(rd, low, preferred_element_type=F32)
-        scan[rows, :] = scan[rows, :] + carried * expd[rows, :] + skips * conv[rows, 0:cw].astype(F32)
-
-    partners(1)
-    for r0 in range(0, n, mt):
-        d = jnp.dot(nbuf[0, r0 : r0 + mt, :], gbuf[0], preferred_element_type=F32)
-        for i in range(1, S):
-            d = d + jnp.dot(nbuf[i, r0 : r0 + mt, :], gbuf[i], preferred_element_type=F32)
-        low = d.astype(BF)
-        extp[raw0 + r0 : raw0 + r0 + mt, :] = low[:, 0:cw].astype(F32)
-        gateb[r0 : r0 + mt, :] = low[:, cw:]
-        if r0 + mt == n:
-            hps[...] = low[mt - raw0 :, 0:cw]
-
-    @pl.when(me < S - 1)
-    def _():
-        halo(hps, hpr, 1).start()
-
-    for b in range(blocks):
-        rows = slice(b * blk, (b + 1) * blk)
+        out_b = scan[rows, :] + carried * expd[rows, :] + skips * conv[rows, 0:cw].astype(F32)
         gt = gateb[rows, :].astype(F32)
-        gated = scan[rows, :] * (gt * jax.nn.sigmoid(gt))
+        gated = out_b * (gt * jax.nn.sigmoid(gt))
         sq_buf[pslot, :, rows] = bt(jnp.ones((8, cw), F32), gated * gated, precision=HIGH)
         sbuf[pslot, rows, :] = (gated * par[0, 16:17, cw : 2 * cw]).astype(BF)
 
-    rows_of = (sbuf, pbuf)
-
-    def rcopy(k, r, way, src=None):
-        to = ({"c_": 1 - c}, {"x_": 1 - x}, {"y_": 1 - y})[way]
-        src = rows_of[k].at[r] if src is None else src
-        return copy(src, rows_of[k].at[r], p_ss.at[(k * T + r) * 3 + way], p_rs.at[k * T + r], **to)
-
-    def qcopy(i):
-        to = ({"c_": 1 - c}, {"x_": 1 - x}, {"x_": 1 - x, "c_": 1 - c}, {})[i]
-        return copy(sq_buf.at[pslot], sq_buf.at[tp], q_ss.at[i], q_rs.at[tp], **{"y_": c, **to})
-
-    def rows_out(k, do):
-        @pl.when(moved)
-        def _():
-            do(rcopy(k, tp, 2, rows_of[k].at[T]))
-
-        @pl.when(kept)
-        def _():
-            do(rcopy(k, tp, 1))
-            do(rcopy(k, tp, 0))
-
-    def rows_on(k, do, wait=True):
-        @pl.when(kept)
-        def _():
-            other = 2 * x + 1 - y
-            if wait:
-                rcopy(k, other, 0).wait_recv()
-            do(rcopy(k, other, 1))
-            do(rcopy(k, other, 0))
-            for r in (2 * (1 - x) + y, 2 * (1 - x) + 1 - y):
-                if wait:
-                    rcopy(k, r, 0).wait_recv()
-                do(rcopy(k, r, 0))
-
-    def squares(do):
-        for i in range(3):
-            do(qcopy(i))
-
-        @pl.when(moved)
-        def _():
-            do(qcopy(3))
-
+    rows_out(0, start)
     squares(start)
-    rows_out(0, start)
-    oslice(5)
-
-    @pl.when(me > 0)
-    def _():
-        halo(hps, hpr, 1).wait_recv()
-        extp[0:raw0, :] = hpr[...].astype(F32)
-
-    @pl.when(me == 0)
-    def _():
-        extp[0:raw0, :] = jnp.zeros((raw0, cw), F32)
-
-    for b in range(blocks):
-        pool(b)
-    rows_out(1, start)
+    olate()
+    oend(0, 0)
+    oend(1, 0)
+    rows_on(1, start)
+    ofar(0, start)
+    oend(1, 1)
+    oend(0, 1)
     rows_on(0, start)
-    oslice(6)
-    rows_on(1, start)
-
+    ofar(1, start)
+    rows_over(1, start)
+    rows_over(0, start)
     @pl.when(moved)
     def _():
         for k in range(2):
@@ -763,8 +930,8 @@
             copy(sq_buf.at[r], sq_buf.at[r], q_ss.at[0], q_rs.at[r], c_=1 - c).wait_recv()
 
     for q in range(T):
-        ref = obuf.at[(1 - y) * T + q]
-        copy(ref, ref, o_ss.at[0], o_rs.at[(1 - y) * T + q], y_=1 - y).wait_recv()
+        i = (1 - y) * T + q
+        copy(obuf.at[i], obuf.at[i], o_ss.at[0], o_rs.at[i], y_=1 - y).wait_recv()
 
     sq = sum(sq_buf[r] for r in range(T))
     rs_row = lax.rsqrt(sq / (cw * T) + EPSILON)
@@ -786,8 +953,8 @@
             pump(k, d, done, wait=False)
         rows_out(k, done)
         rows_on(k, done, wait=False)
-    for q in range(T):
-        omoves(q, done)
+        rows_over(k, done, wait=False)
+    oall(done)
     squares(done)
     acopy(1).wait_send()
     acopy(2).wait_send()
@@ -797,20 +964,20 @@
         acopy(0).wait_send()
         for i in range(4):
             swap(i).wait_send()
-        for f in range(2):
-            aforward(f).wait_send()
+        aforward(0).wait_send()
+
+    @pl.when(kept)
+    def _():
+        aforward(1).wait_send()
 
     @pl.when(jnp.logical_not(hub))
     def _():
         ohub().wait_send()
 
-    for r, bit in enumerate(rounds):
-        copy(xs.at[r], xr.at[r], x_ss.at[r], x_rs.at[r], **xpeer(bit)).wait_send()
-
-    @pl.when(me < S - 1)
-    def _():
-        halo(hvs, hvr, 0).wait_send()
-        halo(hps, hpr, 1).wait_send()
+    xpair().wait_send()
+    xlines(done)
+
+    hsends(done)
 
 
 def fits(S, T, shapes):
@@ -847,16 +1014,15 @@
     vc = cw + 2 * st
     V = pltpu.VMEM
     D = pltpu.SemaphoreType.DMA
-    R = S.bit_length() - 1
     scratch = [
-        V((S + 1, kd + hp, vc), BF), V((S + 1, kd, 2 * cw), BF), V((2 * T + 1, 2 * cw, oc), BF),
+        V((S + 1, kd + hp, vc), BF), V((S + 1, kd, 2 * cw), BF), V((2 * T + 3, 2 * cw, oc), BF),
         V((T + 1, n + 16, da), BF), V((2, cw, cw), BF), V((2, 32, n), F32),
-        V((S, n, kd), BF), V((n + 16, vc), F32), V((n + 16, cw), F32), V((n, cw), BF), V((n, vc), BF),
-        V((16, vc), BF), V((16, vc), BF), V((16, cw), BF), V((16, cw), BF), V((n, cw), F32),
-        V((R, st + 8, cw), F32), V((R, st + 8, cw), F32),
+        V((S, n + 16, kd), BF), V((n + 16, vc), F32), V((n + 16, cw), F32), V((n, cw), BF), V((n, vc), BF),
+        V((T, 16, da), BF), V((n, cw), F32),
+        V((2, st + 8, cw), F32), V((S // 2, st + 8, cw), F32),
         V((T + 1, 8, n), F32), V((T + 1, n, cw), BF), V((T + 1, n, cw), BF), V((n, cw), F32),
-        D((6 * S,)), D((2 * S,)), D((1 + 3 * T,)), D((2 * T,)), D((5,)), D((T,)), D((4,)), D((2,)),
-        D((2,)), D((2,)), D((R,)), D((R,)), D((4,)), D((T,)), D((6 * T,)), D((2 * T,)),
+        D((10 * S,)), D((2 * S,)), D((27,)), D((2 * T + 3,)), D((5,)), D((T,)), D((4,)), D((2,)),
+        D((4,)), D((T,)), D((S // 2,)), D((S // 2,)), D((4,)), D((T,)), D((6 * T,)), D((2 * T,)),
     ]
     return pl.pallas_call(
         functools.partial(mixer_kernel, S, T),

time: 94.8 us -> 90.9 us (0.959)
  the two profiles are of different devices: /device:TPU:1 before, /device:TPU:24 now
where the time goes in v2:
time: 90.9 us; the launch traced here: 90.7 us
  Pallas kernels  87.5 us (96%)
  local copies, waits for them, and re-layouts  3.13 us (3%)
    pallas_call x1, Pallas kernels, fused(): pl.pallas_call(functools.partial(mixer_kernel, S, T), out_shape=jax.Shape...  87.5 us
    unnamed x3, local copies, waits for them, and re-layouts  2.55 us

profile of v2, /device:TPU:24, one launch (start us, length us, event | category | flops | bytes accessed | tf_op | source)
XLA Modules:
  0.0 90.7 jit_solution(1067089064835439185)
XLA Ops:
  0.0 0.0 copy-start
  0.0 0.7 copy-done
  0.7 0.6 broadcast_in_dim.18.gain
  1.3 87.5 %shard_map.190 = bf16[512,512]{1,0:T(8,128)(2,1)} custom-call(bf16[512,512]{1,0:T(8,128)(2,1)} %act.1, bf16[1,512]{1,0:T(2,128)(2,1)} %broadcast_in_dim.18.gain, bf16[256,256]{1,0:T(8,128)(2,1)} %pool_w.1, bf16[256,256]{1,0:T(8,128)(2,1)} %gate_w.1, bf16[256,256]{1,0:T(8,128)(2,1)} %value_w.1, bf16[64,256]{1,0:T(8,128)(2,1)} %bitcast.9, ...), custom_call_target="tpu_custom_call" | custom-call | tf_op jit(solution)/shard_map/pallas_call | solution.py:1027
  88.8 1.9 %copy.22 = bf16[512,512]{1,0:T(8,128)(2,1)} copy(bf16[512,512]{1,0:T(8,128)(2,1)} %shard_map.190) | data formatting | bytes 1048576
Async XLA Ops:
  0.0 0.7 copy-start

commit v3 on v2

--- a/solution.py
+++ b/solution.py
@@ -227,6 +227,9 @@
 def halves(x):
     top = x.astype(BF)
     return top, (x - top.astype(F32)).astype(BF)
+
+
+TWIN = 2
 
 
 def mixer_kernel(
@@ -295,7 +298,9 @@
     vbuf[slot, kd:, :] = jnp.zeros((hp, vc), BF)
     vbuf[slot, kd:, 0:kd] = jnp.dot(pick.astype(BF), step_t[...], preferred_element_type=F32).astype(BF)
     abuf[aslot, 0:n, :] = act[...]
-    abuf[aslot, n : n + 16, :] = jnp.broadcast_to(gain[...].astype(F32), (16, da)).astype(BF)
+    for i in range(gain.shape[0]):
+        g = jnp.broadcast_to(gain[i : i + 1, :].astype(F32), (16, gain.shape[1]))
+        abuf[aslot, n : n + 16, i * gain.shape[1] : (i + 1) * gain.shape[1]] = g.astype(BF)
 
     gbuf[slot, :, 0:cw] = pool_w[...]
     gbuf[slot, :, cw:] = gate_w[...]
@@ -440,13 +445,15 @@
         dst = jnp.where(home, y * T + tq, 2 * T + 1 + turn)
         return copy(obuf.at[2 * T], obuf.at[dst], o_ss.at[0], o_rs.at[dst], c_=1 - c)
 
-    def ocopy(line, j, way):
+    def ocopy(line, j, way, final=False):
         to = (
             {"z_": z + 1}, {"z_": z - 1}, {"z_": z + 2}, {"z_": z - 2},
             {"x_": 1 - x} if line else {"y_": 1 - y},
         )[way]
+        if final and line:
+            to = {"x_": 1 - x, **to}
         i = oslots(line, j)
-        dst = i if way < 4 else y * T + oquarter(j)
+        dst = i if way < 4 and not final else y * T + oquarter(j)
         return copy(obuf.at[i], obuf.at[dst], o_ss.at[1 + (2 * line + j) * 6 + way], o_rs.at[dst], **to)
 
     def owait(line, j):
@@ -462,10 +469,13 @@
             do(ocopy(line, j, 4))
 
     def osend(line, j, do):
-        for way, when in ((2, z == 0), (3, z == Z - 1), (0, middle), (1, middle)):
+        for way, final, when in (
+            (2, False, z == 0), (3, False, z == Z - 1), (0, False, z == 1), (1, True, z == 1),
+            (1, False, z == Z - 2), (0, True, z == Z - 2),
+        ):
             @pl.when(when)
             def _():
-                do(ocopy(line, j, way))
+                do(ocopy(line, j, way, final))
 
     def center(line):
         return 2 * (1 - x) + c if line else tq
@@ -479,7 +489,7 @@
         for way, when in ((0, h < 2), (1, h > 1), (1, h == 0), (0, h == T - 1)):
             @pl.when(when)
             def _():
-                do(ocopy(line, j, way))
+                do(ocopy(line, j, way, True))
 
     def ofrom(j, when=True):
         for line in range(2):
@@ -499,9 +509,9 @@
                     over(line, j, start)
                     across(line, j, start)
 
-    def opass(j):
+    def opass(j, when=True):
         for line in range(2):
-            @pl.when(relays(line))
+            @pl.when(relays(line) & when)
             def _():
                 owait(line, j)
                 orelay(line, j, start)
@@ -518,12 +528,25 @@
                 for j in range(2):
                     across(line, j, start)
 
-    def oend(line, j):
-        @pl.when(jnp.logical_not(hubs[line] | relays(line)))
-        def _():
-            owait(line, j)
-            over(line, j, start)
-            across(line, j, start)
+    def oend(j):
+        @pl.when(jnp.logical_not(hubs[0] | relays(0)))
+        def _():
+            owait(0, j)
+
+            @pl.when(jnp.logical_not(last & (j < TWIN)))
+            def _():
+                across(0, j, start)
+
+    last = ((z == Z - 1) & (x == 0)) | ((z == 0) & (x == 1))
+
+    def otwin(j, do, wait=True):
+        @pl.when(relays(0))
+        def _():
+            i = (1 - y) * T + 2 * x + (1 - y if j == 0 else y)
+            d = copy(obuf.at[i], obuf.at[i], o_ss.at[27 + j], o_rs.at[i], z_=z + 1 - 2 * x)
+            if wait:
+                d.wait_recv()
+            do(d)
 
     def ofar(j, do, wait=True):
         i = y * T + 2 * (1 - x) + (y if j == 0 else 1 - y)
@@ -546,8 +569,16 @@
                 def _():
                     orelay(line, j, do)
 
-                over(line, j, do)
-                across(line, j, do)
+                @pl.when(hubs[line] | relays(line))
+                def _():
+                    over(line, j, do)
+
+                @pl.when(jnp.logical_not(last & (j < TWIN)))
+                def _():
+                    across(line, j, do)
+
+        for j in range(TWIN):
+            otwin(j, do, False)
 
     @pl.when(moved)
     def _():
@@ -561,6 +592,7 @@
         acopy(2).start()
         acopy(0).start()
         swap(2).start()
+        swap(1).start()
 
         @pl.when(jnp.logical_not(hub))
         def _():
@@ -599,7 +631,6 @@
 
     @pl.when(moved)
     def _():
-        swap(1).start()
         swap(3).start()
         arrived(1, me)
         source(1, start)
@@ -609,88 +640,17 @@
         pump(1, 1, start)
 
     partners(0)
-
-    @pl.when(kept)
-    def _():
-        agot(2 * x + 1 - c)
-
-    @pl.when(moved)
-    def _():
-        agot(2 * x + c)
-        agot(2 * (1 - x) + c)
-
-    agot(2 * (1 - x) + 1 - c)
-    hgot()
-
-    ocross()
-    per = da // kd
-    rt = 64
-
-    def norm_rows(parts, r):
-        tot = sum(jnp.sum(p * p, axis=-1, keepdims=True) for p in parts)
-        rs = lax.rsqrt(tot / (da * T) + EPSILON)
-        for t in range(T):
-            g = abuf[t, n : n + 1, :].astype(F32)
-            v = (parts[t] * rs * g).astype(BF)
-            for j in range(per):
-                nbuf[t * per + j, r, :] = v[:, j * kd : (j + 1) * kd]
-
-    def norm_tile(i, _):
-        r = pl.ds(pl.multiple_of(i * rt, rt), rt)
-        norm_rows([abuf[t, r, :].astype(F32) for t in range(T)], r)
-        return 0
-
-    lax.fori_loop(0, n // rt, norm_tile, 0)
-    norm_rows([hbuf[t].astype(F32) for t in range(T)], pl.ds(n, raw0))
-    @pl.when(moved)
-    def _():
-        pump(1, 1, start)
-
-
-    mt = 256
-
-    def tiles():
-        for r0 in range(0, n, mt):
-            yield r0, slice(r0, r0 + mt + raw0 if r0 + mt == n else r0 + mt)
-
-    def keep(ref, r0, low):
-        ref[raw0 + r0 : raw0 + r0 + mt, :] = low[0:mt, :].astype(F32)
-        if low.shape[0] > mt:
-            ref[0:raw0, :] = low[mt:, :].astype(F32)
-
-    for r0, rows in tiles():
-        d = jnp.dot(nbuf[0, rows, :], vbuf[0, 0:kd, :], preferred_element_type=F32)
-        for i in range(1, S):
-            d = d + jnp.dot(nbuf[i, rows, :], vbuf[i, 0:kd, :], preferred_element_type=F32)
-        keep(extv, r0, d.astype(BF))
-
-    sacc = bt(vbuf[0, kd:, 0:kd], nbuf[0, 0:n, :])
-    for i in range(1, S):
-        sacc = sacc + bt(vbuf[i, kd:, 0:kd], nbuf[i, 0:n, :])
-    @pl.when(kept)
-    def _():
-        pump(1, 2, start)
-
-    @pl.when(moved)
-    def _():
-        pump(1, 2, start, when=middle)
-
-    ofrom(0)
-
     @pl.when(moved)
     def _():
         swap(1).wait_recv()
-        swap(3).wait_recv()
 
     def column(row):
         return bt(pick, jnp.broadcast_to(row, (8, heads)), precision=HIGH)[:, 0:1]
 
-    step = sacc + column(par[0, 17:18, 0:heads])
-    step = jnp.maximum(step, 0.0) + jnp.log1p(jnp.exp(-jnp.abs(step)))
-    ld = -jnp.exp(column(par[0, 18:19, 0:heads])) * step + par[0, 0:hp, :]
+    bias_c = column(par[0, 17:18, 0:heads])
+    rate_c = -jnp.exp(column(par[0, 18:19, 0:heads]))
     r_i = lax.broadcasted_iota(jnp.int32, (blk, blk), 0)
     c_i = lax.broadcasted_iota(jnp.int32, (blk, blk), 1)
-    upper = jnp.where(r_i <= c_i, 1.0, 0.0).astype(F32)
     eye = jnp.where(r_i == c_i, 1.0, 0.0).astype(F32)
     lower = r_i >= c_i
     expand = jnp.where(
@@ -703,22 +663,107 @@
     eye_st = jnp.where(
         lax.broadcasted_iota(jnp.int32, (st, st), 0) == lax.broadcasted_iota(jnp.int32, (st, st), 1), 1.0, 0.0
     ).astype(BF)
+
+    def thirds(v):
+        top = v.astype(BF)
+        rest = v - top.astype(F32)
+        mid = rest.astype(BF)
+        return jnp.concatenate([top, mid, (rest - mid.astype(F32)).astype(BF)], axis=1)
+
+    upper = jnp.concatenate([jnp.where(r_i <= c_i, 1.0, 0.0).astype(BF)] * 3, axis=0)
+    row = lax.rem(lax.broadcasted_iota(jnp.int32, (3 * blocks * hp, blocks * cw), 0), blocks * hp)
+    col = lax.broadcasted_iota(jnp.int32, (3 * blocks * hp, blocks * cw), 1)
+    spread = jnp.where(row == (col // cw) * hp + lax.rem(col, cw) // hd, 1.0, 0.0).astype(BF)
+
+
+    @pl.when(kept)
+    def _():
+        agot(2 * x + 1 - c)
+
+    @pl.when(moved)
+    def _():
+        agot(2 * x + c)
+        agot(2 * (1 - x) + c)
+
+    agot(2 * (1 - x) + 1 - c)
+    hgot()
+
+    ocross()
+    ofrom(0, middle & moved)
+    per = da // kd
+    rt = 64
+
+    def norm_rows(parts, r):
+        tot = sum(jnp.sum(p * p, axis=-1, keepdims=True) for p in parts)
+        rs = lax.rsqrt(tot / (da * T) + EPSILON)
+        for t in range(T):
+            g = abuf[t, n : n + 1, :].astype(F32)
+            v = (parts[t] * rs * g).astype(BF)
+            for j in range(per):
+                nbuf[t * per + j, r, :] = v[:, j * kd : (j + 1) * kd]
+
+    def norm_tile(i, _):
+        r = pl.ds(pl.multiple_of(i * rt, rt), rt)
+        norm_rows([abuf[t, r, :].astype(F32) for t in range(T)], r)
+        return 0
+
+    lax.fori_loop(0, n // rt, norm_tile, 0)
+    norm_rows([hbuf[t].astype(F32) for t in range(T)], pl.ds(n, raw0))
+    @pl.when(moved)
+    def _():
+        pump(1, 1, start)
+
+
+    mt = 256
+
+    def tiles():
+        for r0 in range(0, n, mt):
+            yield r0, slice(r0, r0 + mt + raw0 if r0 + mt == n else r0 + mt)
+
+    def keep(ref, r0, low):
+        ref[raw0 + r0 : raw0 + r0 + mt, :] = low[0:mt, :].astype(F32)
+        if low.shape[0] > mt:
+            ref[0:raw0, :] = low[mt:, :].astype(F32)
+
+    for r0, rows in tiles():
+        d = jnp.dot(nbuf[0, rows, :], vbuf[0, 0:kd, :], preferred_element_type=F32)
+        for i in range(1, S):
+            d = d + jnp.dot(nbuf[i, rows, :], vbuf[i, 0:kd, :], preferred_element_type=F32)
+        keep(extv, r0, d.astype(BF))
+
+    sacc = bt(vbuf[0, kd:, 0:kd], nbuf[0, 0:n, :])
+    for i in range(1, S):
+        sacc = sacc + bt(vbuf[i, kd:, 0:kd], nbuf[i, 0:n, :])
+    @pl.when(kept)
+    def _():
+        pump(1, 2, start)
+
+    @pl.when(moved)
+    def _():
+        pump(1, 2, start, when=middle)
+
+    ofrom(0, jnp.logical_not(middle & moved))
+
+    step = sacc + bias_c
+    step = jnp.maximum(step, 0.0) + jnp.log1p(jnp.exp(-jnp.abs(step)))
+    ld = rate_c * step + par[0, 0:hp, :]
+
+    def stacked(v):
+        return jnp.concatenate([v[:, b * blk : (b + 1) * blk] for b in range(blocks)], axis=0)
+
+    cum_r = jnp.dot(thirds(stacked(ld)), upper, preferred_element_type=F32)
+    st_r = stacked(step)
+    cum_c = cum_r.T
+    grown = jnp.exp(cum_c)
+    left = jnp.exp(cum_c[blk - 1 : blk, :] - cum_c) * st_r.T
+    both = jnp.dot(thirds(jnp.concatenate([left, grown], axis=0)), spread, preferred_element_type=F32)
     cum_rs, cum_cs, st_rs, wexps = [], [], [], []
     for b in range(blocks):
-        cols = slice(b * blk, (b + 1) * blk)
-        cum_r = jnp.dot(ld[:, cols], upper, precision=HIGH, preferred_element_type=F32)
-        st_r = step[:, cols]
-        turned = bt(eye, jnp.concatenate([cum_r, st_r], axis=0), precision=HIGH)
-        cum_c = turned[:, 0:hp]
-        w_c = jnp.exp(cum_c[blk - 1 : blk, :] - cum_c) * turned[:, hp:]
-        both = jnp.dot(
-            jnp.concatenate([w_c, jnp.exp(cum_c)], axis=0), expand, precision=HIGH, preferred_element_type=F32
-        )
-        expd[cols, :] = both[blk:, :]
-        wexps.append(both[:blk, :])
-        cum_rs.append(cum_r)
-        cum_cs.append(cum_c)
-        st_rs.append(st_r)
+        expd[b * blk : (b + 1) * blk, :] = both[blk:, b * cw : (b + 1) * cw]
+        wexps.append(both[:blk, b * cw : (b + 1) * cw])
+        cum_rs.append(cum_r[b * hp : (b + 1) * hp, :])
+        cum_cs.append(cum_c[:, b * hp : (b + 1) * hp])
+        st_rs.append(st_r[b * hp : (b + 1) * hp, :])
 
 
     for b in range(blocks):
@@ -841,7 +886,7 @@
         return copy(xs.at[1], xr.at[z], x_ss.at[k], x_rs.at[z], z_=z + k)
 
     def xlines(do):
-        for k in reversed(range(1, Z)):
+        for k in range(1, Z):
             @pl.when(z + k < Z)
             def _():
                 do(xline(k))
@@ -871,20 +916,26 @@
     dec = dec * odec
     put(1)
     xlines(start)
-    ofrom(1)
+    ofrom(1, middle)
 
     for b in range(blocks // 2, blocks):
         inner(b)
-    opass(0)
+    opass(0, kept)
 
     @pl.when(moved)
     def _():
         pump(1, 3, start)
 
+    ofrom(1, jnp.logical_not(middle))
     partners(1)
     gates()
+
+    @pl.when(moved)
+    def _():
+        swap(3).wait_recv()
+
     pools()
-    opass(1)
+    opass(0, moved)
     in_s = jnp.zeros((st, cw), F32)
     for p in range(Z - 1):
         @pl.when(z > p)
@@ -907,17 +958,20 @@
 
     rows_out(0, start)
     squares(start)
+    opass(1)
     olate()
-    oend(0, 0)
-    oend(1, 0)
+    oend(0)
     rows_on(1, start)
     ofar(0, start)
-    oend(1, 1)
-    oend(0, 1)
+    oend(1)
     rows_on(0, start)
+    if TWIN:
+        otwin(0, start)
     ofar(1, start)
     rows_over(1, start)
     rows_over(0, start)
+    if TWIN > 1:
+        otwin(1, start)
     @pl.when(moved)
     def _():
         for k in range(2):
@@ -931,7 +985,11 @@
 
     for q in range(T):
         i = (1 - y) * T + q
-        copy(obuf.at[i], obuf.at[i], o_ss.at[0], o_rs.at[i], y_=1 - y).wait_recv()
+        known = (q == 2 * x + 1 - y) & (TWIN > 0) | (q == 2 * x + y) & (TWIN > 1)
+
+        @pl.when(jnp.logical_not(relays(0) & known))
+        def _():
+            copy(obuf.at[i], obuf.at[i], o_ss.at[0], o_rs.at[i], y_=1 - y).wait_recv()
 
     sq = sum(sq_buf[r] for r in range(T))
     rs_row = lax.rsqrt(sq / (cw * T) + EPSILON)
@@ -1006,7 +1064,7 @@
     oc = out_pool_weight.shape[1]
     hp = 16
     args = (
-        activations, norm_gain[None, :], pool_weight, gate_weight, value_weight, key_weight.T, read_weight.T,
+        activations, norm_gain.reshape(-1, 128), pool_weight, gate_weight, value_weight, key_weight.T, read_weight.T,
         step_weight.T, pool_mix, pool_scale[None, :], taps_value, taps_key, taps_read, step_bias[None, :], decay_log[None, :],
         decay_extra.T, skip_scale[None, :], state_gain[None, :],
         out_pool_weight, out_state_weight,
@@ -1021,7 +1079,7 @@
         V((T, 16, da), BF), V((n, cw), F32),
         V((2, st + 8, cw), F32), V((S // 2, st + 8, cw), F32),
         V((T + 1, 8, n), F32), V((T + 1, n, cw), BF), V((T + 1, n, cw), BF), V((n, cw), F32),
-        D((10 * S,)), D((2 * S,)), D((27,)), D((2 * T + 3,)), D((5,)), D((T,)), D((4,)), D((2,)),
+        D((10 * S,)), D((2 * S,)), D((29,)), D((2 * T + 3,)), D((5,)), D((T,)), D((4,)), D((2,)),
         D((4,)), D((T,)), D((S // 2,)), D((S // 2,)), D((4,)), D((T,)), D((6 * T,)), D((2 * T,)),
     ]
     return pl.pallas_call(

time: 90.9 us -> 82.1 us (0.903)
  the two profiles are of different devices: /device:TPU:24 before, /device:TPU:1 now
where the time goes in v3:
time: 82.1 us; the launch traced here: 81.9 us
  Pallas kernels  80 us (97%)
  local copies, waits for them, and re-layouts  1.87 us (2%)
    pallas_call x1, Pallas kernels, fused(): pl.pallas_call(functools.partial(mixer_kernel, S, T), out_shape=jax.Shape...  80 us
    unnamed x1, local copies, waits for them, and re-layouts  1.87 us

profile of v3, /device:TPU:1, one launch (start us, length us, event | category | flops | bytes accessed | tf_op | source)
XLA Modules:
  0.0 81.9 jit_solution(3456858196459759323)
XLA Ops:
  0.0 80.0 %shard_map.190 = bf16[512,512]{1,0:T(8,128)(2,1)} custom-call(bf16[512,512]{1,0:T(8,128)(2,1)} %act.1, bf16[4,128]{1,0:T(4,128)(2,1)} %bitcast.14, bf16[256,256]{1,0:T(8,128)(2,1)} %pool_w.1, bf16[256,256]{1,0:T(8,128)(2,1)} %gate_w.1, bf16[256,256]{1,0:T(8,128)(2,1)} %value_w.1, bf16[64,256]{1,0:T(8,128)(2,1)} %bitcast.10, bf16[64,256]{1,0:T(8,128)(2,1)} %bitcast.11, ...), custom_call_target="tpu_custom_call" | custom-call | tf_op jit(solution)/shard_map/pallas_call | solution.py:1085
  80.0 1.9 %copy.22 = bf16[512,512]{1,0:T(8,128)(2,1)} copy(bf16[512,512]{1,0:T(8,128)(2,1)} %shard_map.190) | data formatting | bytes 1048576

commit v4 on v3

--- a/solution.py
+++ b/solution.py
@@ -405,9 +405,22 @@
         to = ({"c_": y}, {"x_": 1 - x, "c_": y}, {"y_": 1 - y, "c_": y})[way]
         return copy(abuf.at[aslot], abuf.at[tq], a_ss.at[way], a_rs.at[tq], **to)
 
+    head = n // 2 + 16
+
     def aforward(i):
-        t, to = ((2 * x + 1 - c, {"x_": 1 - x}), (2 * (1 - x) + c, {"y_": 1 - y}))[i]
-        return copy(abuf.at[t], abuf.at[t], a_ss.at[3 + i], a_rs.at[t], **to)
+        t, rows, rs, to = (
+            (2 * x + 1 - c, pl.ds(0, n + 16), None, {"x_": 1 - x}),
+            (2 * (1 - x) + c, pl.ds(0, head), None, {"y_": 1 - y}),
+            (2 * x + c, pl.ds(head, n + 16 - head), T, {"x_": 1 - x}),
+        )[i]
+        ref = abuf.at[t, rows]
+        return copy(ref, ref, a_ss.at[3 + i], a_rs.at[t if rs is None else rs], **to)
+
+    def afar():
+        t = 2 * (1 - x) + c
+        for rows, rs in ((pl.ds(0, head), t), (pl.ds(head, n + 16 - head), T)):
+            ref = abuf.at[t, rows]
+            copy(ref, ref, a_ss.at[0], a_rs.at[rs], x_=1 - x).wait_recv()
 
     def agot(t):
         copy(abuf.at[t], abuf.at[t], a_ss.at[0], a_rs.at[t], x_=1 - x).wait_recv()
@@ -521,12 +534,10 @@
                 def _():
                     across(line, j, start)
 
-    def olate():
-        for line in range(2):
-            @pl.when(relays(line) & moved)
-            def _():
-                for j in range(2):
-                    across(line, j, start)
+    def olate(j):
+        @pl.when(relays(0) & moved)
+        def _():
+            across(0, j, start)
 
     def oend(j):
         @pl.when(jnp.logical_not(hubs[0] | relays(0)))
@@ -626,6 +637,11 @@
         aforward(0).start()
 
     pump(0, 2, start)
+
+    @pl.when(moved)
+    def _():
+        agot(2 * x + c)
+        aforward(2).start()
 
     pump(0, 3, start)
 
@@ -682,8 +698,7 @@
 
     @pl.when(moved)
     def _():
-        agot(2 * x + c)
-        agot(2 * (1 - x) + c)
+        afar()
 
     agot(2 * (1 - x) + 1 - c)
     hgot()
@@ -882,8 +897,26 @@
     def xpair():
         return copy(xs.at[0], xr.at[Z - 1], x_ss.at[0], x_rs.at[Z - 1], c_=1 - c)
 
+    def lanes(who):
+        return pl.ds(pl.multiple_of(who * (cw // 2), cw // 2), cw // 2)
+
     def xline(k):
-        return copy(xs.at[1], xr.at[z], x_ss.at[k], x_rs.at[z], z_=z + k)
+        return copy(xs.at[1, :, lanes(c)], xr.at[z, :, lanes(c)], x_ss.at[k], x_rs.at[z], z_=z + k)
+
+    def xshare(p, who):
+        ref = xr.at[p, :, lanes(who)]
+        return copy(ref, ref, x_ss.at[Z + p], x_rs.at[Z + p], c_=1 - c)
+
+    def xshares(do):
+        for p in range(Z - 1):
+            @pl.when(z > p)
+            def _():
+                do(p)
+
+    def xgot(p):
+        ref = xr.at[p, :, lanes(c)]
+        copy(ref, ref, x_ss.at[1], x_rs.at[p], c_=1 - c).wait_recv()
+        xshare(p, c).start()
 
     def xlines(do):
         for k in range(1, Z):
@@ -936,11 +969,12 @@
 
     pools()
     opass(0, moved)
+    xshares(xgot)
     in_s = jnp.zeros((st, cw), F32)
     for p in range(Z - 1):
         @pl.when(z > p)
         def _():
-            copy(xs.at[1], xr.at[p], x_ss.at[1], x_rs.at[p], c_=1 - c).wait_recv()
+            xshare(p, 1 - c).wait_recv()
 
         in_s = jnp.where(z > p, in_s * xr[p, st : st + 1, :] + xr[p, 0:st, :], in_s)
     in_s = in_s * own_d + own_s
@@ -958,8 +992,9 @@
 
     rows_out(0, start)
     squares(start)
+    olate(0)
     opass(1)
-    olate()
+    olate(1)
     oend(0)
     rows_on(1, start)
     ofar(0, start)
@@ -969,19 +1004,44 @@
         otwin(0, start)
     ofar(1, start)
     rows_over(1, start)
-    rows_over(0, start)
     if TWIN > 1:
         otwin(1, start)
-    @pl.when(moved)
-    def _():
-        for k in range(2):
+    def rows_here(k):
+        @pl.when(moved)
+        def _():
             for r in range(T):
                 rcopy(k, r, 0).wait_recv()
 
+    def product(k, family, rows):
+        part = slice(cw, 2 * cw) if k == 0 else slice(0, cw)
+        p = jnp.dot(rows_of[k][0, rows, :], obuf[family * T, part, :], preferred_element_type=F32)
+        for q in range(1, T):
+            p = p + jnp.dot(rows_of[k][q, rows, :], obuf[family * T + q, part, :], preferred_element_type=F32)
+        return p
+
+    def spots(family):
+        return pl.ds(pl.multiple_of(family * oc, oc), oc)
+
+    rows_here(1)
+    for r0 in range(0, n, mt):
+        scan[r0 : r0 + mt, 0:oc] = product(1, y, slice(r0, r0 + mt))
+    rows_over(0, start)
+    rows_here(0)
     for r in range(T):
         @pl.when((tp != r) | moved)
         def _():
             copy(sq_buf.at[r], sq_buf.at[r], q_ss.at[0], q_rs.at[r], c_=1 - c).wait_recv()
+
+    sq = sum(sq_buf[r] for r in range(T))
+    rs_row = lax.rsqrt(sq / (cw * T) + EPSILON)
+    rs_cols = [bt(eye, rs_row[:, b * blk : (b + 1) * blk], precision=HIGH)[:, 0:1] for b in range(blocks)]
+
+    def scales(r0):
+        return jnp.concatenate(rs_cols[r0 // blk : (r0 + mt) // blk], axis=0)
+
+    for r0 in range(0, n, mt):
+        rows = slice(r0, r0 + mt)
+        out[rows, spots(y)] = (scan[rows, 0:oc] + scales(r0) * product(0, y, rows)).astype(out.dtype)
 
     for q in range(T):
         i = (1 - y) * T + q
@@ -991,19 +1051,10 @@
         def _():
             copy(obuf.at[i], obuf.at[i], o_ss.at[0], o_rs.at[i], y_=1 - y).wait_recv()
 
-    sq = sum(sq_buf[r] for r in range(T))
-    rs_row = lax.rsqrt(sq / (cw * T) + EPSILON)
-    rs_cols = [bt(eye, rs_row[:, b * blk : (b + 1) * blk], precision=HIGH)[:, 0:1] for b in range(blocks)]
     for r0 in range(0, n, mt):
         rows = slice(r0, r0 + mt)
-        rs = jnp.concatenate(rs_cols[r0 // blk : (r0 + mt) // blk], axis=0)
-        for j in range(2):
-            p = jnp.dot(pbuf[0, rows, :], obuf[j * T, 0:cw, :], preferred_element_type=F32)
-            s = jnp.dot(sbuf[0, rows, :], obuf[j * T, cw:, :], preferred_element_type=F32)
-            for q in range(1, T):
-                p = p + jnp.dot(pbuf[q, rows, :], obuf[j * T + q, 0:cw, :], preferred_element_type=F32)
-                s = s + jnp.dot(sbuf[q, rows, :], obuf[j * T + q, cw:, :], preferred_element_type=F32)
-            out[rows, j * oc : (j + 1) * oc] = (p + rs * s).astype(out.dtype)
+        p = product(1, 1 - y, rows)
+        out[rows, spots(1 - y)] = (p + scales(r0) * product(0, 1 - y, rows)).astype(out.dtype)
 
     for k in range(2):
         source(k, done)
@@ -1023,6 +1074,7 @@
         for i in range(4):
             swap(i).wait_send()
         aforward(0).wait_send()
+        aforward(2).wait_send()
 
     @pl.when(kept)
     def _():
@@ -1034,6 +1086,7 @@
 
     xpair().wait_send()
     xlines(done)
+    xshares(lambda p: xshare(p, c).wait_send())
 
     hsends(done)
 
@@ -1049,7 +1102,7 @@
         T == 4 == POOL_GROUPS and S == 2 * T and st == SSM_STATE and taps <= 8 and heads <= 8
         and cw == heads * SSM_STATE and n % 256 == 0 and n % SCAN_BLOCK == 0 and n >= 2 * cw
         and oc % 128 == 0 and kd % 128 == 0 and da % kd == 0 and da * T == kd * S and kd <= cw + 2 * st
-        and cw % 128 == 0 and oc * 2 == da
+        and cw % 256 == 0 and oc * 2 == da and oc <= cw
     )
 
 
@@ -1079,8 +1132,8 @@
         V((T, 16, da), BF), V((n, cw), F32),
         V((2, st + 8, cw), F32), V((S // 2, st + 8, cw), F32),
         V((T + 1, 8, n), F32), V((T + 1, n, cw), BF), V((T + 1, n, cw), BF), V((n, cw), F32),
-        D((10 * S,)), D((2 * S,)), D((29,)), D((2 * T + 3,)), D((5,)), D((T,)), D((4,)), D((2,)),
-        D((4,)), D((T,)), D((S // 2,)), D((S // 2,)), D((4,)), D((T,)), D((6 * T,)), D((2 * T,)),
+        D((10 * S,)), D((2 * S,)), D((29,)), D((2 * T + 3,)), D((6,)), D((T + 1,)), D((4,)), D((2,)),
+        D((4,)), D((T,)), D((S,)), D((S,)), D((4,)), D((T,)), D((6 * T,)), D((2 * T,)),
     ]
     return pl.pallas_call(
         functools.partial(mixer_kernel, S, T),

time: 82.1 us -> 81.3 us (level)
  no operation moved by 1% of the time
where the time goes in v4:
time: 81.3 us; the launch traced here: 81.1 us
  Pallas kernels  79.2 us (97%)
  local copies, waits for them, and re-layouts  1.87 us (2%)
    pallas_call x1, Pallas kernels, fused(): pl.pallas_call(functools.partial(mixer_kernel, S, T), out_shape=jax.Shape...  79.2 us
    unnamed x1, local copies, waits for them, and re-layouts  1.87 us

profile of v4, /device:TPU:1, one launch (start us, length us, event | category | flops | bytes accessed | tf_op | source)
XLA Modules:
  0.0 81.1 jit_solution(1684974725876703527)
XLA Ops:
  0.0 79.2 %shard_map.190 = bf16[512,512]{1,0:T(8,128)(2,1)} custom-call(bf16[512,512]{1,0:T(8,128)(2,1)} %act.1, bf16[4,128]{1,0:T(4,128)(2,1)} %bitcast.14, bf16[256,256]{1,0:T(8,128)(2,1)} %pool_w.1, bf16[256,256]{1,0:T(8,128)(2,1)} %gate_w.1, bf16[256,256]{1,0:T(8,128)(2,1)} %value_w.1, bf16[64,256]{1,0:T(8,128)(2,1)} %bitcast.10, bf16[64,256]{1,0:T(8,128)(2,1)} %bitcast.11, ...), custom_call_target="tpu_custom_call" | custom-call | tf_op jit(solution)/shard_map/pallas_call | solution.py:1138
  79.2 1.9 %copy.22 = bf16[512,512]{1,0:T(8,128)(2,1)} copy(bf16[512,512]{1,0:T(8,128)(2,1)} %shard_map.190) | data formatting | bytes 1048576
